TPU v7x, 32 devices: a whole 2x2x4 slice. The times are simulated.
32 devices in a mesh: sp: 4 (over y, x), tp: 8 (over z, core).
Axes of the slice: x: 2, y: 2, z: 4, core: 2. Of those that a mesh axis runs over, the one named last changes fastest.
Arguments:
- inputs: bfloat16 [2, 2048, 4096], P(None, 'sp', 'tp'), may hold values from -16 to 16
- in_gain: float32 [4096], replicated, may hold values from 0.1 to 1.9
- key_weight: bfloat16 [4096, 2048], P(None, 'tp'), may hold values from -0.0014648438 to 0.0014648438
- value_weight: bfloat16 [4096, 4096], P(None, 'tp'), may hold values from -0.09375 to 0.09375
- decay_down: bfloat16 [4096, 32], replicated, may hold values from -0.09375 to 0.09375
- decay_up: bfloat16 [32, 2048], replicated, may hold values from -1 to 1
- decay_bias: float32 [2048], replicated, may hold values from 0 to 10
- new_query: bfloat16 [2, 2048], P(None, 'tp'), may hold values from -6 to 6
- out_gain: float32 [256], replicated, may hold values from 0.1 to 1.9
Outputs:
- cache: bfloat16 [2, 16, 128, 256], P(None, 'tp', 'sp')
- read: bfloat16 [2, 4096], P(None, 'tp')
All inputs are finite; a program needn't handle non-finite values.
Results may differ from a plain program's by a relative error of at most 0.0085.
Values may be sent and summed in bfloat16 or wider, within the bound.
A program may use at most 64 MiB of HBM per device.

v0:
```python
import functools

import jax
import jax.numpy as jnp
from jax import lax
from jax.experimental import pallas as pl
from jax.experimental.pallas import tpu as pltpu
from jax.sharding import PartitionSpec as P

DK = 128
DV = 256
CHUNK = 256
AHEAD = 2
MESH = pl.DeviceIdType.MESH
F32 = jnp.float32
BF16 = jnp.bfloat16


def split3(value):
    high = value.astype(BF16)
    rest = value - high.astype(F32)
    middle = rest.astype(BF16)
    low = (rest - middle.astype(F32)).astype(BF16)
    return high, middle, low


def kernel(
    n_sp,
    n_z,
    x_ref,
    gain_hbm,
    wk_hbm,
    wv_hbm,
    wd_hbm,
    up_hbm,
    bias_hbm,
    query_hbm,
    cache_ref,
    parts_ref,
    xbuf,
    wk,
    wv,
    wd,
    up,
    bias,
    gain_ref,
    query_ref,
    acc_k,
    acc_v,
    acc_l,
    acc_s,
    state,
    carry,
    tots,
    terms,
    landed,
    reads,
    load_sem,
    own_sem,
    line_send,
    relay_send,
    pair_send,
    recv,
    tot_send,
    tot_recv,
    term_send,
    term_recv,
    read_send,
    read_recv,
):
    seqs, span, feats = x_ref.shape
    per_seq = span // CHUNK
    chunks = seqs * per_seq
    heads = wk_hbm.shape[1] // DK
    share = DK // n_sp
    model = n_z * 2 * feats
    sp = lax.axis_index("sp")
    tp = lax.axis_index("tp")
    z = tp // 2
    c = lax.rem(tp, 2)
    key_cols = heads * DK

    first = pl.multiple_of(tp * key_cols, key_cols)
    loads = [
        pltpu.make_async_copy(wk_hbm, wk, load_sem.at[0]),
        pltpu.make_async_copy(wv_hbm, wv, load_sem.at[1]),
        pltpu.make_async_copy(wd_hbm, wd, load_sem.at[2]),
        pltpu.make_async_copy(up_hbm.at[:, pl.ds(first, key_cols)], up, load_sem.at[3]),
        pltpu.make_async_copy(bias_hbm.at[:, pl.ds(first, key_cols)], bias, load_sem.at[4]),
        pltpu.make_async_copy(gain_hbm, gain_ref, load_sem.at[5]),
        pltpu.make_async_copy(query_hbm, query_ref, load_sem.at[6]),
    ]

    def chunk_rows(j):
        seq = j // per_seq
        start = (per_seq - 1 - lax.rem(j, per_seq)) * CHUNK
        return seq, pl.multiple_of(start, CHUNK)

    def own_copy(j):
        seq, start = chunk_rows(j)
        return pltpu.make_async_copy(
            x_ref.at[seq, pl.ds(start, CHUNK), :], xbuf.at[j, z, c], own_sem.at[j]
        )

    def line_copy(j, there):
        return pltpu.make_async_remote_copy(
            src_ref=xbuf.at[j, z, c],
            dst_ref=xbuf.at[j, z, c],
            send_sem=line_send.at[j, there],
            recv_sem=recv.at[j, z, c],
            device_id={"tp": there * 2 + c},
            device_id_type=MESH,
        )

    def relay_copy(j, zz, end):
        return pltpu.make_async_remote_copy(
            src_ref=xbuf.at[j, zz, c],
            dst_ref=xbuf.at[j, zz, c],
            send_sem=relay_send.at[j, zz],
            recv_sem=recv.at[j, zz, c],
            device_id={"tp": end * 2 + c},
            device_id_type=MESH,
        )

    ends = ((0, 1), (n_z - 1, n_z - 2))

    def each_end(act):
        for end, inner in ends:

            @pl.when(z == inner)
            def _():
                act(end)

    def each_inner(act):
        for there in range(1, n_z - 1):

            @pl.when(z != there)
            def _():
                act(there)

    def each_relayed(zz, act):
        for end, inner in ends:
            beyond = zz > inner if end == 0 else zz < inner

            @pl.when((z == inner) & beyond)
            def _():
                act(end)

    def pair_copy(j, zz, cc):
        return pltpu.make_async_remote_copy(
            src_ref=xbuf.at[j, zz, cc],
            dst_ref=xbuf.at[j, zz, cc],
            send_sem=pair_send.at[j, zz],
            recv_sem=recv.at[j, zz, cc],
            device_id={"tp": tp + 1 - 2 * c},
            device_id_type=MESH,
        )

    for j in range(chunks):
        own_copy(j).start()
    for load in loads:
        load.start()

    barrier = pltpu.get_barrier_semaphore()
    at_end = (z == 0) | (z == n_z - 1)
    for there in range(n_z):
        met = z != there
        if n_z > 2 and there in (0, n_z - 1):
            met = met & jnp.logical_not(at_end)

        @pl.when(met)
        def _():
            pl.semaphore_signal(
                barrier, inc=1, device_id={"tp": there * 2 + c}, device_id_type=MESH
            )

    pl.semaphore_signal(barrier, inc=1, device_id={"tp": tp + 1 - 2 * c}, device_id_type=MESH)
    for off in range(1, n_sp):
        pl.semaphore_signal(
            barrier, inc=1, device_id={"sp": lax.rem(sp + off, n_sp)}, device_id_type=MESH
        )
    far = jnp.where(at_end, 1, 0) if n_z > 2 else 0
    pl.semaphore_wait(barrier, n_z - 1 + n_sp - far)

    def send_end(j):
        each_end(lambda end: line_copy(j, end).start())

    for j in range(chunks):
        own_copy(j).wait()
        each_inner(lambda there: line_copy(j, there).start())
        if j < AHEAD:
            send_end(j)
        pair_copy(j, z, c).start()
    for load in loads:
        load.wait()

    def clear_chunk():
        acc_k[...] = jnp.zeros_like(acc_k)
        acc_v[...] = jnp.zeros_like(acc_v)
        acc_l[...] = jnp.zeros_like(acc_l)
        acc_s[...] = jnp.zeros_like(acc_s)

    def add_shard(j, zz, cc):
        slot = zz * 2 + cc
        wide = xbuf[j, zz, cc].astype(F32)
        scaled = (wide * gain_ref[slot]).astype(BF16)
        rows = pl.ds(pl.multiple_of(slot * feats, feats), feats)
        acc_k[...] += jnp.dot(scaled, wk[rows, :], preferred_element_type=F32)
        acc_v[...] += jnp.dot(scaled, wv[rows, :], preferred_element_type=F32)
        acc_l[...] += lax.dot_general(
            scaled, wd[:, rows], (((1,), (1,)), ((), ())), preferred_element_type=F32
        )
        square = wide * wide
        total = square[:, 0:128]
        for lane in range(128, feats, 128):
            total = total + square[:, lane : lane + 128]
        acc_s[...] += total

    def gather_step(j, i):
        away = (i + 1) // 2
        way = 1 - 2 * lax.rem(i, 2)
        zz = z + way * away

        @pl.when((zz >= 0) & (zz < n_z))
        def _():
            @pl.when(i > 0)
            def _():
                relay_copy(j, zz, 0).wait_recv()
                each_relayed(zz, lambda end: relay_copy(j, zz, end).start())
                pair_copy(j, zz, c).start()

            add_shard(j, zz, c)
            pair_copy(j, zz, 1 - c).wait_recv()
            add_shard(j, zz, 1 - c)

    def finish_chunk(j):
        seq = j // per_seq

        @pl.when(lax.rem(j, per_seq) == 0)
        def _():
            carry[...] = jnp.zeros_like(carry)
            state[seq] = jnp.zeros(state.shape[1:], F32)

        inv_rms = lax.rsqrt(jnp.sum(acc_s[...], axis=1, keepdims=True) / model + 1e-06)
        low_rank = acc_l[...] * inv_rms
        gate = bias[...] + jnp.dot(
            jnp.concatenate(split3(low_rank), axis=1),
            jnp.concatenate([up[...]] * 3, axis=0),
            preferred_element_type=F32,
        )
        log_decay = (jnp.minimum(gate, 0.0) - jnp.log1p(jnp.exp(-jnp.abs(gate)))) / 16.0
        later = (
            lax.broadcasted_iota(jnp.int32, (CHUNK, CHUNK), 1)
            > lax.broadcasted_iota(jnp.int32, (CHUNK, CHUNK), 0)
        ).astype(BF16)
        suffix = carry[...] + jnp.dot(
            jnp.concatenate([later] * 3, axis=1),
            jnp.concatenate(split3(log_decay), axis=0),
            preferred_element_type=F32,
        )
        carry[...] = carry[...] + jnp.sum(log_decay, axis=0, keepdims=True)
        last = lax.rem(j, per_seq) == per_seq - 1

        @pl.when(last)
        def _():
            send_total(seq)

        keys = (acc_k[...] * inv_rms).astype(BF16).astype(F32)
        weighted = keys * jnp.exp(suffix)
        values = (acc_v[...] * inv_rms).astype(BF16)
        for h in range(heads):
            part = weighted[:, h * DK : (h + 1) * DK].T.astype(BF16)
            rows = pl.ds(h * DK, DK)
            state[seq, rows, :] = state[seq, rows, :] + jnp.dot(
                part, values[:, h * DV : (h + 1) * DV], preferred_element_type=F32
            )

        @pl.when(last)
        def _():
            send_terms(seq)

    peers = [lax.rem(sp + off, n_sp) for off in range(1, n_sp)]

    def tot_copy(seq, peer, slot):
        return pltpu.make_async_remote_copy(
            src_ref=tots.at[seq, sp],
            dst_ref=tots.at[seq, slot],
            send_sem=tot_send.at[seq, peer],
            recv_sem=tot_recv.at[seq, slot],
            device_id={"sp": peer},
            device_id_type=MESH,
        )

    def term_copy(seq, peer, slot):
        return pltpu.make_async_remote_copy(
            src_ref=terms.at[seq, peer],
            dst_ref=landed.at[seq, slot],
            send_sem=term_send.at[seq, peer],
            recv_sem=term_recv.at[seq, slot],
            device_id={"sp": peer},
            device_id_type=MESH,
        )

    def read_copy(seq, peer, slot):
        return pltpu.make_async_remote_copy(
            src_ref=reads.at[seq, sp],
            dst_ref=reads.at[seq, slot],
            send_sem=read_send.at[seq, peer],
            recv_sem=read_recv.at[seq, slot],
            device_id={"sp": peer},
            device_id_type=MESH,
        )

    def send_total(seq):
        tots[seq, sp] = carry[...]
        for peer in peers:
            tot_copy(seq, peer, sp).start()

    def send_terms(seq):
        for h in range(heads):
            for p in range(n_sp):
                row = h * DK + p * share
                terms[seq, p, h] = state[seq, row : row + share, :].astype(BF16)
        for peer in peers:
            term_copy(seq, peer, sp).start()

    def send_reads(seq):
        chosen = (
            lax.broadcasted_iota(jnp.int32, (share, DK), 0) + sp * share
            == lax.broadcasted_iota(jnp.int32, (share, DK), 1)
        )

        def column(row):
            return jnp.sum(jnp.where(chosen, row, 0.0), axis=1, keepdims=True)

        for peer in peers:
            tot_copy(seq, peer, peer).wait_recv()
        after = jnp.zeros((1, key_cols), F32)
        factors = [None] * n_sp
        for p in reversed(range(n_sp)):
            decay = jnp.exp(after)
            factors[p] = [column(decay[:, h * DK : (h + 1) * DK]) for h in range(heads)]
            after = after + tots[seq, p]
        for peer in peers:
            term_copy(seq, peer, peer).wait_recv()
        own = [
            state[seq, pl.ds(pl.multiple_of(h * DK + sp * share, share), share), :]
            for h in range(heads)
        ]
        sums = []
        for h in range(heads):
            total = jnp.zeros((share, DV), F32)
            for p in range(n_sp):
                block = jnp.where(p == sp, own[h], landed[seq, p, h].astype(F32))
                total = total + factors[p][h] * block
            sums.append(total)
        for h in range(heads):
            cache = sums[h].astype(BF16)
            cache_ref[seq, h] = cache
            queries = query_ref[seq : seq + 1, h * DK : (h + 1) * DK].astype(F32)
            reads[seq, sp, h : h + 1, :] = jnp.sum(
                column(queries) * cache.astype(F32), axis=0, keepdims=True
            )
        for peer in peers:
            read_copy(seq, peer, sp).start()

    def give_read(seq):
        for peer in peers:
            read_copy(seq, peer, peer).wait_recv()
        parts_ref[seq] = reads[seq]

    def drain(j, _):
        pair_copy(j, z, c).wait_send()
        each_inner(lambda there: line_copy(j, there).wait_send())
        each_end(lambda end: line_copy(j, end).wait_send())

        def inner(i, _):
            away = (i + 1) // 2
            way = 1 - 2 * lax.rem(i, 2)
            zz = z + way * away

            @pl.when((zz >= 0) & (zz < n_z))
            def _():
                each_relayed(zz, lambda end: relay_copy(j, zz, end).wait_send())
                pair_copy(j, zz, c).wait_send()

            return 0

        lax.fori_loop(1, 2 * n_z - 1, inner, 0)
        return 0

    def chunk_step(j, _):
        @pl.when(j + AHEAD < chunks)
        def _():
            send_end(j + AHEAD)

        clear_chunk()

        def inner(i, _):
            gather_step(j, i)
            return 0

        lax.fori_loop(0, 2 * n_z - 1, inner, 0)
        finish_chunk(j)

        @pl.when((j > 0) & (j < chunks - 1))
        def _():
            drain(j - 1, 0)

        return 0

    lax.fori_loop(0, chunks - 1, chunk_step, 0)
    for seq in range(seqs - 1):
        send_reads(seq)
    chunk_step(chunks - 1, 0)
    if chunks > 1:
        drain(chunks - 2, 0)
    drain(chunks - 1, 0)
    send_reads(seqs - 1)
    for seq in range(seqs):
        give_read(seq)
    for seq in range(seqs):
        for peer in peers:
            tot_copy(seq, peer, sp).wait_send()
            term_copy(seq, peer, sp).wait_send()
            read_copy(seq, peer, sp).wait_send()


def norm_kernel(cache_in, parts_ref, gain_ref, cache_ref, read_ref):
    cache_ref[...] = cache_in[...]
    seqs, n_sp, heads, _ = parts_ref.shape
    for seq in range(seqs):
        readout = parts_ref[seq, 0]
        for p in range(1, n_sp):
            readout = readout + parts_ref[seq, p]
        mean = jnp.mean(readout * readout, axis=-1, keepdims=True)
        normed = (readout * lax.rsqrt(mean + 1e-06) * gain_ref[...]).astype(BF16)
        for h in range(heads):
            read_ref[seq : seq + 1, h * DV : (h + 1) * DV] = normed[h : h + 1, :]


def per_device(
    n_sp,
    n_z,
    inputs,
    in_gain,
    key_weight,
    value_weight,
    decay_down,
    decay_up,
    decay_bias,
    new_query,
    out_gain,
):
    seqs, span, feats = inputs.shape
    model, key_cols = key_weight.shape
    value_cols = value_weight.shape[1]
    rank = decay_down.shape[1]
    heads = key_cols // DK
    chunks = seqs * (span // CHUNK)
    share = DK // n_sp
    vmem = pl.BlockSpec(memory_space=pltpu.VMEM)
    hbm = pl.BlockSpec(memory_space=pl.ANY)
    dma = pltpu.SemaphoreType.DMA
    cache, parts = pl.pallas_call(
        functools.partial(kernel, n_sp, n_z),
        out_shape=(
            jax.ShapeDtypeStruct((seqs, heads, share, DV), BF16),
            jax.ShapeDtypeStruct((seqs, n_sp, heads, DV), F32),
        ),
        in_specs=[hbm] * 8,
        out_specs=(vmem, vmem),
        scratch_shapes=[
            pltpu.VMEM((chunks, n_z, 2, CHUNK, feats), BF16),
            pltpu.VMEM((model, key_cols), BF16),
            pltpu.VMEM((model, value_cols), BF16),
            pltpu.VMEM((rank, model), BF16),
            pltpu.VMEM((rank, key_cols), BF16),
            pltpu.VMEM((1, key_cols), F32),
            pltpu.VMEM((2 * n_z, 1, feats), F32),
            pltpu.VMEM((seqs, key_cols), BF16),
            pltpu.VMEM((CHUNK, key_cols), F32),
            pltpu.VMEM((CHUNK, value_cols), F32),
            pltpu.VMEM((CHUNK, rank), F32),
            pltpu.VMEM((CHUNK, 128), F32),
            pltpu.VMEM((seqs, key_cols, DV), F32),
            pltpu.VMEM((1, key_cols), F32),
            pltpu.VMEM((seqs, n_sp, 1, key_cols), F32),
            pltpu.VMEM((seqs, n_sp, heads, share, DV), BF16),
            pltpu.VMEM((seqs, n_sp, heads, share, DV), BF16),
            pltpu.VMEM((seqs, n_sp, heads, DV), F32),
            dma((7,)),
            dma((chunks,)),
            dma((chunks, n_z)),
            dma((chunks, n_z)),
            dma((chunks, n_z)),
            dma((chunks, n_z, 2)),
            dma((seqs, n_sp)),
            dma((seqs, n_sp)),
            dma((seqs, n_sp)),
            dma((seqs, n_sp)),
            dma((seqs, n_sp)),
            dma((seqs, n_sp)),
        ],
        compiler_params=pltpu.CompilerParams(
            collective_id=0, has_side_effects=True, vmem_limit_bytes=60 * 1024 * 1024
        ),
    )(
        inputs,
        in_gain.reshape(2 * n_z, 1, feats),
        key_weight,
        value_weight,
        decay_down.T,
        decay_up,
        decay_bias.reshape(1, -1),
        new_query,
    )
    return pl.pallas_call(
        norm_kernel,
        out_shape=(
            jax.ShapeDtypeStruct((seqs, heads, share, DV), BF16),
            jax.ShapeDtypeStruct((seqs, heads * DV), BF16),
        ),
        in_specs=[vmem, vmem, vmem],
        out_specs=(vmem, vmem),
    )(cache, parts, out_gain.reshape(1, -1))


def solution(mesh):
    in_specs = (
        P(None, "sp", "tp"),
        P(),
        P(None, "tp"),
        P(None, "tp"),
        P(),
        P(),
        P(),
        P(None, "tp"),
        P(),
    )
    out_specs = (P(None, "tp", "sp", None), P(None, "tp"))
    return jax.shard_map(
        functools.partial(per_device, mesh.shape["sp"], mesh.shape["tp"] // 2),
        mesh=mesh,
        in_specs=in_specs,
        out_specs=out_specs,
        check_vma=False,
    )
```

profile of v0, /device:TPU:0, one launch (start us, length us, event | category | flops | bytes accessed | tf_op | source)
XLA Modules:
  0.0 87.2 jit_solution(438994898594504486)
XLA Ops:
  0.6 85.1 %shard_map.104 = (bf16[2,2,32,256]{3,2,1,0:T(8,128)(2,1)}, f32[2,4,2,256]{3,2,1,0:T(2,128)}) custom-call(bf16[2,512,512]{2,1,0:T(8,128)(2,1)} %x_ref.1, f32[8,1,512]{2,1,0:T(1,128)} %bitcast.5, bf16[4096,256]{1,0:T(8,128)(2,1)} %wk_hbm.1, bf16[4096,512]{1,0:T(8,128)(2,1)} %wv_hbm.1, bf16[32,4096]{1,0:T(8,128)(2,1)} %bitcast.4, bf16[32,2048]{1,0:T(8,128)(2,1)} %up_hbm.1, ...), custom_call_target="tpu_custom_call" | custom-call | tf_op jit(solution)/shard_map/pallas_call | solution.py:465
  85.7 1.5 %shard_map.105 = (bf16[2,2,32,256]{3,2,1,0:T(8,128)(2,1)}, bf16[2,512]{1,0:T(2,128)(2,1)}) custom-call(bf16[2,2,32,256]{3,2,1,0:T(8,128)(2,1)} %get-tuple-element.4.cache_in, f32[2,4,2,256]{3,2,1,0:T(2,128)} %get-tuple-element.5.parts_ref, f32[1,256]{1,0:T(1,128)} %bitcast.7), custom_call_target="tpu_custom_call" | custom-call | tf_op jit(solution)/shard_map/pallas_call | solution.py:518
where the time goes:
time: 87.4 us; the launch traced here: 87.2 us
  Pallas kernels  86.6 us (99%)
    pallas_call x1, Pallas kernels, per_device(): pl.pallas_call(functools.partial(kernel, n_sp, n_z), out_shape=(jax.Shape...  85.1 us

commit v1 on v0

v1 whole, which is shorter than its diff:
```python
import functools

import jax
import jax.numpy as jnp
from jax import lax
from jax.experimental import pallas as pl
from jax.experimental.pallas import tpu as pltpu
from jax.sharding import PartitionSpec as P

DK = 128
DV = 256
CHUNK = 128
LENT_SEQ = 0
MESH = pl.DeviceIdType.MESH
F32 = jnp.float32
BF16 = jnp.bfloat16


def split3(value):
    high = value.astype(BF16)
    rest = value - high.astype(F32)
    middle = rest.astype(BF16)
    low = (rest - middle.astype(F32)).astype(BF16)
    return high, middle, low


def lends(n_sp, n_z, heads):
    return n_z >= 4 and n_sp == 2 * heads


def kernel(
    n_sp,
    n_z,
    x_ref,
    gain_hbm,
    wk_hbm,
    wv_hbm,
    wd_hbm,
    up_hbm,
    bias_hbm,
    query_hbm,
    cache_ref,
    parts_ref,
    xbuf,
    wk,
    wv,
    wd,
    up,
    bias,
    gain_ref,
    query_ref,
    acc_k,
    acc_v,
    acc_l,
    acc_s,
    state,
    carry,
    fade,
    scale,
    tots,
    terms,
    landed,
    reads,
    load_sem,
    own_sem,
    hop_send,
    pair_send,
    recv,
    tot_send,
    tot_recv,
    term_send,
    term_recv,
    read_send,
    read_recv,
    lent_x=None,
    lent_wk=None,
    lent_wv=None,
    lent_up=None,
    lent_bias=None,
    lent_k=None,
    lent_v=None,
    lent_l=None,
    lent_s=None,
    lent_fade=None,
    lent_scale=None,
    hint=None,
    lent_terms=None,
    lent_tots=None,
    back_terms=None,
    back_tots=None,
    hint_send=None,
    hint_recv=None,
    lent_x_send=None,
    lent_x_recv=None,
    lent_w_send=None,
    lent_w_pair=None,
    lent_w_recv=None,
    back_send=None,
    back_recv=None,
):
    seqs, span, feats = x_ref.shape
    per_seq = span // CHUNK
    chunks = seqs * per_seq
    heads = wk_hbm.shape[1] // DK
    share = DK // n_sp
    slots = 2 * n_z
    model = slots * feats
    lend = lends(n_sp, n_z, heads)
    lent = LENT_SEQ * per_seq + per_seq - 1
    tail = chunks - 1
    sp = lax.axis_index("sp")
    tp = lax.axis_index("tp")
    z = tp // 2
    c = lax.rem(tp, 2)
    key_cols = heads * DK
    at_end = (z == 0) | (z == n_z - 1)
    low_half = z < n_z // 2
    end = jnp.where(low_half, 0, n_z - 1)
    inner = jnp.where(low_half, 1, n_z - 2)
    at_inner = z == inner
    flip = jnp.where(low_half, 1, -1)
    reach = jnp.where(low_half, n_z - 1 - z, z)
    final_step = 2 * reach - 1
    lender = at_end & (c == sp // 2)
    peers = [lax.rem(sp + off, n_sp) for off in range(1, n_sp)]

    first = pl.multiple_of(tp * key_cols, key_cols)
    loads = [
        pltpu.make_async_copy(wk_hbm, wk, load_sem.at[0]),
        pltpu.make_async_copy(wv_hbm, wv, load_sem.at[1]),
        pltpu.make_async_copy(wd_hbm, wd, load_sem.at[2]),
        pltpu.make_async_copy(up_hbm.at[:, pl.ds(first, key_cols)], up, load_sem.at[3]),
        pltpu.make_async_copy(bias_hbm.at[:, pl.ds(first, key_cols)], bias, load_sem.at[4]),
        pltpu.make_async_copy(gain_hbm, gain_ref, load_sem.at[5]),
        pltpu.make_async_copy(query_hbm, query_ref, load_sem.at[6]),
    ]
    if lend:
        other = pl.multiple_of((end * 2 * heads + sp) * DK, DK)
        loads += [
            pltpu.make_async_copy(up_hbm.at[:, pl.ds(other, DK)], lent_up, load_sem.at[7]),
            pltpu.make_async_copy(bias_hbm.at[:, pl.ds(other, DK)], lent_bias, load_sem.at[8]),
        ]

    def stage_w(act):
        head = lax.rem(sp, 2)
        for n, (src, dst, width) in enumerate(((wk_hbm, lent_wk, DK), (wv_hbm, lent_wv, DV))):
            columns = pl.ds(pl.multiple_of(head * width, width), width)
            act(pltpu.make_async_copy(src.at[:, columns], dst, load_sem.at[9 + n]))

    def chunk_rows(j):
        seq = j // per_seq
        start = (per_seq - 1 - lax.rem(j, per_seq)) * CHUNK
        return seq, pl.multiple_of(start, CHUNK)

    def own_copy(j):
        seq, start = chunk_rows(j)
        return pltpu.make_async_copy(
            x_ref.at[seq, pl.ds(start, CHUNK), :], xbuf.at[j, z, c], own_sem.at[j]
        )

    def hop_copy(j, zz, way):
        return pltpu.make_async_remote_copy(
            src_ref=xbuf.at[j, zz, c],
            dst_ref=xbuf.at[j, zz, c],
            send_sem=hop_send.at[j, zz, way],
            recv_sem=recv.at[j, zz, c],
            device_id={"tp": (z + 2 * way - 1) * 2 + c},
            device_id_type=MESH,
        )

    def pair_copy(j, zz, cc):
        return pltpu.make_async_remote_copy(
            src_ref=xbuf.at[j, zz, cc],
            dst_ref=xbuf.at[j, zz, cc],
            send_sem=pair_send.at[j, zz],
            recv_sem=recv.at[j, zz, cc],
            device_id={"tp": tp + 1 - 2 * c},
            device_id_type=MESH,
        )

    def each_way(j, zz, act):
        for way, edge in ((0, 0), (1, n_z - 1)):
            there = z + 2 * way - 1
            beyond = (zz >= z) if way == 0 else (zz <= z)
            wanted = (z != edge) & beyond
            if lend:
                wanted = wanted & ((j != lent) | (there != edge))

            @pl.when(wanted)
            def _():
                act(hop_copy(j, zz, way))

    def held(j, zz):
        return at_inner & (j == tail) & (flip * (zz - z) > 0)

    def used(j):
        if not lend:
            return j >= 0
        return (j != lent) | jnp.logical_not(at_end)

    def lend_x(zz, act):
        for n, peer in enumerate(peers):
            act(
                pltpu.make_async_remote_copy(
                    src_ref=xbuf.at[lent, zz, c],
                    dst_ref=lent_x.at[lax.rem(sp, 2), zz, c],
                    send_sem=lent_x_send.at[zz, n],
                    recv_sem=lent_x_recv.at[lax.rem(sp, 2), zz, c],
                    device_id={"sp": peer, "tp": z * 2 + sp // 2},
                    device_id_type=MESH,
                )
            )

    def lend_w(slot, act):
        rows = pl.ds(pl.multiple_of(slot * feats, feats), feats)
        for n, both in enumerate((lent_wk, lent_wv)):
            act(
                pltpu.make_async_remote_copy(
                    src_ref=both.at[rows, :],
                    dst_ref=both.at[rows, :],
                    send_sem=lent_w_send.at[n, slot],
                    recv_sem=lent_w_recv.at[n, slot],
                    device_id={"tp": inner * 2 + c},
                    device_id_type=MESH,
                )
            )

    def pair_w(slot, act):
        rows = pl.ds(pl.multiple_of(slot * feats, feats), feats)
        for n, both in enumerate((lent_wk, lent_wv)):
            act(
                pltpu.make_async_remote_copy(
                    src_ref=both.at[rows, :],
                    dst_ref=both.at[rows, :],
                    send_sem=lent_w_pair.at[n, slot],
                    recv_sem=lent_w_recv.at[n, slot],
                    device_id={"tp": tp + 1 - 2 * c},
                    device_id_type=MESH,
                )
            )

    def hint_copy():
        return pltpu.make_async_remote_copy(
            src_ref=hint,
            dst_ref=hint,
            send_sem=hint_send,
            recv_sem=hint_recv,
            device_id={"tp": end * 2 + c},
            device_id_type=MESH,
        )

    def give_back(n, p):
        lines = pl.ds(2 * c, 2)
        src, dst = ((lent_tots, back_tots), (lent_terms.at[p], back_terms))[n]
        return pltpu.make_async_remote_copy(
            src_ref=src,
            dst_ref=dst.at[lax.rem(sp, 2), lines],
            send_sem=back_send.at[n, p],
            recv_sem=back_recv.at[n, lax.rem(sp, 2), c],
            device_id={"sp": p, "tp": end * 2 + sp // 2},
            device_id_type=MESH,
        )

    for j in range(chunks):
        own_copy(j).start()
    for load in loads:
        load.start()
    if lend:
        pl.when(lender)(lambda: stage_w(lambda copy: copy.start()))

    barrier = pltpu.get_barrier_semaphore()

    def greet(ahead, device):
        @pl.when(ahead)
        def _():
            pl.semaphore_signal(barrier, inc=1, device_id=device, device_id_type=MESH)

    close = at_end | at_inner if lend else False
    apart = jnp.logical_not(close)
    for way, edge in ((0, 0), (1, n_z - 1)):
        there = z + 2 * way - 1
        met = z != edge
        if lend:
            met = met & jnp.logical_not(close & ((there == end) | (there == inner)))
        greet(met, {"tp": there * 2 + c})
    if lend:
        for p in range(n_sp):
            for plane in (end, inner):
                for core in range(2):
                    known = close & ((p != sp) | (plane != z) | (core != c))
                    greet(known, {"sp": p, "tp": plane * 2 + core})
        greet(apart, {"tp": tp + 1 - 2 * c})
        for peer in peers:
            greet(apart, {"sp": peer})
        far = jnp.where(close, 4 * n_sp - 1 + jnp.where(at_inner, 1, 0), 2 + n_sp)
    else:
        greet(tp >= 0, {"tp": tp + 1 - 2 * c})
        for peer in peers:
            greet(tp >= 0, {"sp": peer})
        far = n_sp + jnp.where(z > 0, 1, 0) + jnp.where(z < n_z - 1, 1, 0)

    acc_k[...] = jnp.zeros_like(acc_k)
    acc_v[...] = jnp.zeros_like(acc_v)
    acc_l[...] = jnp.zeros_like(acc_l)
    acc_s[...] = jnp.zeros_like(acc_s)
    if lend:

        @pl.when(at_inner)
        def _():
            lent_k[...] = jnp.zeros_like(lent_k)
            lent_v[...] = jnp.zeros_like(lent_v)
            lent_l[...] = jnp.zeros_like(lent_l)
            lent_s[...] = jnp.zeros_like(lent_s)

        @pl.when(jnp.logical_not(at_end))
        def _():
            back_terms[...] = jnp.zeros_like(back_terms)
            back_tots[...] = jnp.zeros_like(back_tots)

    pl.semaphore_wait(barrier, far)

    def open_chunk(j, _):
        own_copy(j).wait()
        each_way(j, z, lambda copy: copy.start())

        @pl.when(used(j))
        def _():
            pair_copy(j, z, c).start()

        return 0

    lax.fori_loop(0, chunks, open_chunk, 0)
    if lend:

        @pl.when(at_inner)
        def _():
            lend_x(z, lambda copy: copy.start())

    for load in loads:
        load.wait()
    if lend:
        pl.when(lender)(lambda: stage_w(lambda copy: copy.wait()))

    def project(scaled, slot, rows, weights, accs):
        deep = pl.ds(pl.multiple_of(slot * feats, feats), feats)
        for weight, acc in zip(weights, accs):
            acc[rows] += jnp.dot(scaled, weight[deep, :], preferred_element_type=F32)

    def reduce_rank(wide, scaled, slot, rows, acc_rank, acc_square):
        deep = pl.ds(pl.multiple_of(slot * feats, feats), feats)
        acc_rank[rows] += lax.dot_general(
            scaled, wd[:, deep], (((1,), (1,)), ((), ())), preferred_element_type=F32
        )
        square = wide * wide
        total = square[:, 0:128]
        for lane in range(128, feats, 128):
            total = total + square[:, lane : lane + 128]
        acc_square[rows] += total

    def add_shard(j, zz, cc):
        slot = zz * 2 + cc
        wide = xbuf[j, zz, cc].astype(F32)
        scaled = (wide * gain_ref[slot]).astype(BF16)
        project(scaled, slot, j, (wk, wv), (acc_k, acc_v))
        reduce_rank(wide, scaled, slot, j, acc_l, acc_s)

    def source(i):
        away = (i + 1) // 2
        return z + flip * (2 * lax.rem(i, 2) - 1) * away

    def visit(i, j):
        zz = source(i)

        @pl.when(used(j))
        def _():
            @pl.when(i > 0)
            def _():
                pair_copy(j, zz, c).wait_recv()
                if lend:

                    @pl.when(jnp.logical_not(held(j, zz)))
                    def _():
                        each_way(j, zz, lambda copy: copy.start())

                else:
                    each_way(j, zz, lambda copy: copy.start())
                pair_copy(j, zz, c).start()
                if lend:

                    @pl.when(at_inner & (j == lent))
                    def _():
                        lend_x(zz, lambda copy: copy.start())

            add_shard(j, zz, c)

    def complete(i, j):
        zz = source(i)

        @pl.when(used(j))
        def _():
            pair_copy(j, zz, 1 - c).wait_recv()
            add_shard(j, zz, 1 - c)

    def normed(acc_rank, acc_square, rows):
        inv_rms = lax.rsqrt(jnp.sum(acc_square[rows], axis=1, keepdims=True) / model + 1e-06)
        return acc_rank[rows] * inv_rms, inv_rms

    def faded(low_rank, gate_up, gate_bias, start):
        gate = gate_bias[...] + jnp.dot(
            jnp.concatenate(split3(low_rank), axis=1),
            jnp.concatenate([gate_up[...]] * 3, axis=0),
            preferred_element_type=F32,
        )
        log_decay = (jnp.minimum(gate, 0.0) - jnp.log1p(jnp.exp(-jnp.abs(gate)))) / 16.0
        later = (
            lax.broadcasted_iota(jnp.int32, (CHUNK, CHUNK), 1)
            > lax.broadcasted_iota(jnp.int32, (CHUNK, CHUNK), 0)
        ).astype(BF16)
        suffix = start + jnp.dot(
            jnp.concatenate([later] * 3, axis=1),
            jnp.concatenate(split3(log_decay), axis=0),
            preferred_element_type=F32,
        )
        return jnp.exp(suffix), start + jnp.sum(log_decay, axis=0, keepdims=True)

    def fade_chunk(j, low_rank, inv_rms):
        weights, total = faded(low_rank, up, bias, carry[...])
        fade[...] = weights
        scale[...] = jnp.broadcast_to(inv_rms, scale.shape)
        carry[...] = total

        @pl.when(lax.rem(j, per_seq) == per_seq - 1)
        def _():
            send_total(j // per_seq)

    def finish_chunk(j):
        seq = j // per_seq

        @pl.when(lax.rem(j, per_seq) == 0)
        def _():
            carry[...] = jnp.zeros_like(carry)
            state[seq] = jnp.zeros(state.shape[1:], F32)

        last = lax.rem(j, per_seq) == per_seq - 1

        @pl.when(used(j))
        def _():
            known = at_end & (j == tail) if lend else j < 0

            @pl.when(jnp.logical_not(known))
            def _():
                fade_chunk(j, *normed(acc_l, acc_s, j))

            inv_rms = scale[:, :1]
            keys = (acc_k[j] * inv_rms).astype(BF16).astype(F32)
            weighted = keys * fade[...]
            values = (acc_v[j] * inv_rms).astype(BF16)
            for h in range(heads):
                part = weighted[:, h * DK : (h + 1) * DK].T.astype(BF16)
                rows = pl.ds(h * DK, DK)
                state[seq, rows, :] = state[seq, rows, :] + jnp.dot(
                    part, values[:, h * DV : (h + 1) * DV], preferred_element_type=F32
                )

        if lend:

            @pl.when(jnp.logical_not(used(j)))
            def _():
                send_total(seq)

        @pl.when(last)
        def _():
            send_terms(seq)

    def tot_copy(seq, peer, slot):
        return pltpu.make_async_remote_copy(
            src_ref=tots.at[seq, sp],
            dst_ref=tots.at[seq, slot],
            send_sem=tot_send.at[seq, peer],
            recv_sem=tot_recv.at[seq, slot],
            device_id={"sp": peer},
            device_id_type=MESH,
        )

    def term_copy(seq, peer, slot):
        return pltpu.make_async_remote_copy(
            src_ref=terms.at[seq, peer],
            dst_ref=landed.at[seq, slot],
            send_sem=term_send.at[seq, peer],
            recv_sem=term_recv.at[seq, slot],
            device_id={"sp": peer},
            device_id_type=MESH,
        )

    def read_copy(seq, peer, slot):
        return pltpu.make_async_remote_copy(
            src_ref=reads.at[seq, sp],
            dst_ref=reads.at[seq, slot],
            send_sem=read_send.at[seq, peer],
            recv_sem=read_recv.at[seq, slot],
            device_id={"sp": peer},
            device_id_type=MESH,
        )

    def send_total(seq):
        tots[seq, sp] = carry[...]
        for peer in peers:
            tot_copy(seq, peer, sp).start()

    def send_terms(seq):
        for h in range(heads):
            for p in range(n_sp):
                row = h * DK + p * share
                terms[seq, p, h] = state[seq, row : row + share, :].astype(BF16)
        for peer in peers:
            term_copy(seq, peer, sp).start()

    def await_back(n):
        both = (back_tots, back_terms)[n]
        for head in range(heads):
            for core in range(2):
                lines = pl.ds(2 * core, 2)
                pltpu.make_async_remote_copy(
                    src_ref=both.at[head, lines],
                    dst_ref=both.at[head, lines],
                    send_sem=back_send.at[n, 0],
                    recv_sem=back_recv.at[n, head, core],
                    device_id={"tp": inner * 2 + c},
                    device_id_type=MESH,
                ).wait_recv()

    def column(row, begin, size):
        chosen = (
            lax.broadcasted_iota(jnp.int32, (size, DK), 0) + begin
            == lax.broadcasted_iota(jnp.int32, (size, DK), 1)
        )
        return jnp.sum(jnp.where(chosen, row, 0.0), axis=1, keepdims=True)

    def query(seq, h):
        return query_ref[seq : seq + 1, h * DK : (h + 1) * DK].astype(F32)

    def send_parts(seq):
        for peer in peers:
            tot_copy(seq, peer, peer).wait_recv()
        for h in range(heads):
            after = jnp.zeros((1, DK), F32)
            for p in range(n_sp):
                total = tots[seq, p][:, h * DK : (h + 1) * DK]
                after = after + jnp.where(p > sp, total, 0.0)
            asked = column(query(seq, h) * jnp.exp(after), 0, DK)
            reads[seq, sp, h : h + 1, :] = jnp.sum(
                asked * state[seq, h * DK : (h + 1) * DK, :], axis=0, keepdims=True
            )
        for peer in peers:
            read_copy(seq, peer, sp).start()

    def sum_terms(seq, loaned):
        if loaned:
            pl.when(at_end)(lambda: await_back(0))
        after = [jnp.zeros((1, DK), F32)] * heads
        factors = [None] * n_sp
        back_factors = [None] * n_sp
        for p in reversed(range(n_sp)):
            factors[p] = [column(jnp.exp(row), sp * share, share) for row in after]
            after = [after[h] + tots[seq, p][:, h * DK : (h + 1) * DK] for h in range(heads)]
            if loaned:
                back_factors[p] = [column(jnp.exp(row), sp * share, share) for row in after]
                after = [after[h] + back_tots[h, p] for h in range(heads)]
        for peer in peers:
            term_copy(seq, peer, peer).wait_recv()
        if loaned:
            pl.when(at_end)(lambda: await_back(1))
        for h in range(heads):
            own = state[seq, pl.ds(pl.multiple_of(h * DK + sp * share, share), share), :]
            total = jnp.zeros((share, DV), F32)
            for p in range(n_sp):
                block = jnp.where(p == sp, own, landed[seq, p, h].astype(F32))
                total = total + factors[p][h] * block
                if loaned:
                    total = total + back_factors[p][h] * back_terms[h, p].astype(F32)
            cache_ref[seq, h] = total.astype(BF16)

    def send_reads(seq):
        for peer in peers:
            tot_copy(seq, peer, peer).wait_recv()
        sum_terms(seq, True)
        for h in range(heads):
            reads[seq, sp, h : h + 1, :] = jnp.sum(
                column(query(seq, h), sp * share, share) * cache_ref[seq, h].astype(F32),
                axis=0,
                keepdims=True,
            )
        for peer in peers:
            read_copy(seq, peer, sp).start()

    def give_read(seq):
        for peer in peers:
            read_copy(seq, peer, peer).wait_recv()
        parts_ref[seq] = reads[seq]

    def lent_scaled(slot):
        wide = lent_x[:, slot // 2, lax.rem(slot, 2)].reshape(2 * CHUNK, feats).astype(F32)
        return wide, (wide * gain_ref[slot]).astype(BF16)

    def work_off():
        every = slice(None)

        def collect(slot, _):
            zz, cc = slot // 2, lax.rem(slot, 2)
            for line in range(2):
                mine = 2 * c + line == sp

                @pl.when(mine)
                def _():
                    lent_x[line, zz, cc] = xbuf[lent, zz, cc]

                @pl.when(jnp.logical_not(mine))
                def _():
                    pltpu.make_async_remote_copy(
                        src_ref=lent_x.at[line, zz, cc],
                        dst_ref=lent_x.at[line, zz, cc],
                        send_sem=lent_x_send.at[zz, 0],
                        recv_sem=lent_x_recv.at[line, zz, cc],
                        device_id={"tp": tp + 1 - 2 * c},
                        device_id_type=MESH,
                    ).wait_recv()

            wide, scaled = lent_scaled(slot)
            reduce_rank(wide, scaled, slot, every, lent_l, lent_s)
            return 0

        lax.fori_loop(0, slots, collect, 0)
        blocks = [slice(line * CHUNK, (line + 1) * CHUNK) for line in range(2)]
        for line, rows in enumerate(blocks):
            low_rank, inv_rms = normed(lent_l, lent_s, rows)
            weights, total = faded(low_rank, lent_up, lent_bias, jnp.zeros((1, DK), F32))
            lent_fade[rows] = weights
            lent_scale[rows] = jnp.broadcast_to(inv_rms, weights.shape)
            lent_tots[line] = total
        for p in range(n_sp):
            give_back(0, p).start()

        def multiply(slot, _):
            pair_w(slot, lambda copy: copy.wait_recv())

            @pl.when(c == sp // 2)
            def _():
                pair_w(slot, lambda copy: copy.start())

            _, scaled = lent_scaled(slot)
            project(scaled, slot, every, (lent_wk, lent_wv), (lent_k, lent_v))
            return 0

        lax.fori_loop(0, slots, multiply, 0)
        for line, rows in enumerate(blocks):
            inv_rms = lent_scale[rows, :1]
            keys = (lent_k[rows] * inv_rms).astype(BF16).astype(F32)
            weighted = keys * lent_fade[rows]
            values = (lent_v[rows] * inv_rms).astype(BF16)
            block = jnp.dot(weighted.T.astype(BF16), values, preferred_element_type=F32)
            for p in range(n_sp):
                lent_terms[p, line] = block[p * share : (p + 1) * share].astype(BF16)
        for p in range(n_sp):
            give_back(1, p).start()

    def send_hint():
        low_rank, inv_rms = normed(acc_l, acc_s, tail)
        spread = jnp.broadcast_to(inv_rms, (CHUNK, 128 - low_rank.shape[1]))
        hint[...] = jnp.concatenate([low_rank, spread], axis=1).T[: hint.shape[0]]
        hint_copy().start()

        def release(i, _):
            zz = source(i)

            @pl.when((zz >= 0) & (zz < n_z) & held(tail, zz))
            def _():
                each_way(tail, zz, lambda copy: copy.start())

            return 0

        lax.fori_loop(1, final_step + 1, release, 0)

    def take_hint():
        hint_copy().wait_recv()
        rank = wd.shape[0]
        full = jnp.concatenate(
            [hint[...], jnp.zeros((128 - hint.shape[0], CHUNK), F32)], axis=0
        ).T
        fade_chunk(tail, full[:, :rank], full[:, rank : rank + 1])

        overdue(visit)

    def overdue(act):
        def one(i, _):
            zz = source(i)

            @pl.when((zz >= 0) & (zz < n_z))
            def _():
                act(i, tail)

            return 0

        lax.fori_loop(2, final_step, one, 0)

    steps = 2 * n_z - 2

    def ready(i, j):
        zz = source(i)
        inside = (zz >= 0) & (zz < n_z)
        if lend:
            inside = inside & jnp.logical_not(at_end & (j == tail) & (i > 1) & (i < final_step))
        return inside

    def settle(i, j):
        final = i == final_step
        closing = final & (j == tail)

        @pl.when(ready(i, j))
        def _():
            if lend:
                pl.when(at_end & closing)(lambda: overdue(complete))
            complete(i, j)
            if lend:
                pl.when(at_inner & closing)(send_hint)

            @pl.when(final)
            def _():
                finish_chunk(j)

    def step(t, _):
        i, j = t // chunks, lax.rem(t, chunks)
        last_i, last_j = (t - 1) // chunks, lax.rem(t - 1, chunks)
        early = at_end & (i == final_step) & (j == tail) if lend else t < 0
        if lend:

            @pl.when(early)
            def _():
                settle(last_i, last_j)
                take_hint()

            @pl.when(lender & (t == 2 * chunks))
            def _():
                def lend_slot(slot, _):
                    lend_w(slot, lambda copy: copy.start())
                    return 0

                lax.fori_loop(0, slots, lend_slot, 0)

        @pl.when(ready(i, j))
        def _():
            visit(i, j)

        @pl.when(jnp.logical_not(early))
        def _():
            settle(last_i, last_j)

        return 0

    visit(0, 0)
    lax.fori_loop(1, steps * chunks, step, 0)
    settle(steps - 1, chunks - 1)
    if lend:

        @pl.when(at_inner)
        def _():
            send_reads(LENT_SEQ)
            work_off()

    rest = [seq for seq in range(seqs) if not (lend and seq == LENT_SEQ)]
    for seq in rest:
        send_parts(seq)
    if lend:
        pl.when(jnp.logical_not(at_inner))(lambda: send_reads(LENT_SEQ))
    for seq in rest:
        sum_terms(seq, False)

    def drain(i, _):
        zz = source(i)

        @pl.when((zz >= 0) & (zz < n_z))
        def _():
            def inside(j, _):
                @pl.when((i == 0) | used(j))
                def _():
                    each_way(j, zz, lambda copy: copy.wait_send())

                @pl.when(used(j))
                def _():
                    pair_copy(j, zz, c).wait_send()

                return 0

            lax.fori_loop(0, chunks, inside, 0)

        return 0

    lax.fori_loop(0, 2 * n_z - 2, drain, 0)
    if lend:

        def drain_slot(slot, _):
            pl.when(lender)(lambda: lend_w(slot, lambda copy: copy.wait_send()))

            @pl.when(at_inner & (c == sp // 2))
            def _():
                pair_w(slot, lambda copy: copy.wait_send())

            return 0

        lax.fori_loop(0, slots, drain_slot, 0)

        @pl.when(at_inner)
        def _():
            for zz in range(n_z):
                lend_x(zz, lambda copy: copy.wait_send())
            for p in range(n_sp):
                give_back(0, p).wait_send()
                give_back(1, p).wait_send()
            hint_copy().wait_send()

    for seq in range(seqs):
        give_read(seq)
    for seq in range(seqs):
        for peer in peers:
            tot_copy(seq, peer, sp).wait_send()
            term_copy(seq, peer, sp).wait_send()
            read_copy(seq, peer, sp).wait_send()


def norm_kernel(cache_in, parts_ref, gain_ref, cache_ref, read_ref):
    cache_ref[...] = cache_in[...]
    seqs, n_sp, heads, _ = parts_ref.shape
    for seq in range(seqs):
        readout = parts_ref[seq, 0]
        for p in range(1, n_sp):
            readout = readout + parts_ref[seq, p]
        mean = jnp.mean(readout * readout, axis=-1, keepdims=True)
        normed = (readout * lax.rsqrt(mean + 1e-06) * gain_ref[...]).astype(BF16)
        for h in range(heads):
            read_ref[seq : seq + 1, h * DV : (h + 1) * DV] = normed[h : h + 1, :]


def per_device(
    n_sp,
    n_z,
    inputs,
    in_gain,
    key_weight,
    value_weight,
    decay_down,
    decay_up,
    decay_bias,
    new_query,
    out_gain,
):
    seqs, span, feats = inputs.shape
    model, key_cols = key_weight.shape
    value_cols = value_weight.shape[1]
    rank = decay_down.shape[1]
    heads = key_cols // DK
    chunks = seqs * (span // CHUNK)
    share = DK // n_sp
    slots = 2 * n_z
    vmem = pl.BlockSpec(memory_space=pltpu.VMEM)
    hbm = pl.BlockSpec(memory_space=pl.ANY)
    dma = pltpu.SemaphoreType.DMA
    lent = []
    if lends(n_sp, n_z, heads):
        lent = [
            pltpu.VMEM((2, n_z, 2, CHUNK, feats), BF16),
            pltpu.VMEM((model, DK), BF16),
            pltpu.VMEM((model, DV), BF16),
            pltpu.VMEM((rank, DK), BF16),
            pltpu.VMEM((1, DK), F32),
            pltpu.VMEM((2 * CHUNK, DK), F32),
            pltpu.VMEM((2 * CHUNK, DV), F32),
            pltpu.VMEM((2 * CHUNK, rank), F32),
            pltpu.VMEM((2 * CHUNK, 128), F32),
            pltpu.VMEM((2 * CHUNK, DK), F32),
            pltpu.VMEM((2 * CHUNK, DK), F32),
            pltpu.VMEM((rank + 8, CHUNK), F32),
            pltpu.VMEM((n_sp, 2, share, DV), BF16),
            pltpu.VMEM((2, 1, DK), F32),
            pltpu.VMEM((heads, n_sp, share, DV), BF16),
            pltpu.VMEM((heads, n_sp, 1, DK), F32),
            dma,
            dma,
            dma((n_z, n_sp - 1)),
            dma((2, n_z, 2)),
            dma((2, slots)),
            dma((2, slots)),
            dma((2, slots)),
            dma((2, n_sp)),
            dma((2, heads, 2)),
        ]
    cache, parts = pl.pallas_call(
        functools.partial(kernel, n_sp, n_z),
        out_shape=(
            jax.ShapeDtypeStruct((seqs, heads, share, DV), BF16),
            jax.ShapeDtypeStruct((seqs, n_sp, heads, DV), F32),
        ),
        in_specs=[hbm] * 8,
        out_specs=(vmem, vmem),
        scratch_shapes=[
            pltpu.VMEM((chunks, n_z, 2, CHUNK, feats), BF16),
            pltpu.VMEM((model, key_cols), BF16),
            pltpu.VMEM((model, value_cols), BF16),
            pltpu.VMEM((rank, model), BF16),
            pltpu.VMEM((rank, key_cols), BF16),
            pltpu.VMEM((1, key_cols), F32),
            pltpu.VMEM((slots, 1, feats), F32),
            pltpu.VMEM((seqs, key_cols), BF16),
            pltpu.VMEM((chunks, CHUNK, key_cols), F32),
            pltpu.VMEM((chunks, CHUNK, value_cols), F32),
            pltpu.VMEM((chunks, CHUNK, rank), F32),
            pltpu.VMEM((chunks, CHUNK, 128), F32),
            pltpu.VMEM((seqs, key_cols, DV), F32),
            pltpu.VMEM((1, key_cols), F32),
            pltpu.VMEM((CHUNK, key_cols), F32),
            pltpu.VMEM((CHUNK, 128), F32),
            pltpu.VMEM((seqs, n_sp, 1, key_cols), F32),
            pltpu.VMEM((seqs, n_sp, heads, share, DV), BF16),
            pltpu.VMEM((seqs, n_sp, heads, share, DV), BF16),
            pltpu.VMEM((seqs, n_sp, heads, DV), F32),
            dma((11,)),
            dma((chunks,)),
            dma((chunks, n_z, 2)),
            dma((chunks, n_z)),
            dma((chunks, n_z, 2)),
            dma((seqs, n_sp)),
            dma((seqs, n_sp)),
            dma((seqs, n_sp)),
            dma((seqs, n_sp)),
            dma((seqs, n_sp)),
            dma((seqs, n_sp)),
        ]
        + lent,
        compiler_params=pltpu.CompilerParams(
            collective_id=0, has_side_effects=True, vmem_limit_bytes=60 * 1024 * 1024
        ),
    )(
        inputs,
        in_gain.reshape(slots, 1, feats),
        key_weight,
        value_weight,
        decay_down.T,
        decay_up,
        decay_bias.reshape(1, -1),
        new_query,
    )
    return pl.pallas_call(
        norm_kernel,
        out_shape=(
            jax.ShapeDtypeStruct((seqs, heads, share, DV), BF16),
            jax.ShapeDtypeStruct((seqs, heads * DV), BF16),
        ),
        in_specs=[vmem, vmem, vmem],
        out_specs=(vmem, vmem),
    )(cache, parts, out_gain.reshape(1, -1))


def solution(mesh):
    in_specs = (
        P(None, "sp", "tp"),
        P(),
        P(None, "tp"),
        P(None, "tp"),
        P(),
        P(),
        P(),
        P(None, "tp"),
        P(),
    )
    out_specs = (P(None, "tp", "sp", None), P(None, "tp"))
    return jax.shard_map(
        functools.partial(per_device, mesh.shape["sp"], mesh.shape["tp"] // 2),
        mesh=mesh,
        in_specs=in_specs,
        out_specs=out_specs,
        check_vma=False,
    )
```

time: 87.4 us -> 80.7 us (0.923)
  Pallas kernels: 86.6 us -> 79.9 us
    pallas_call x1, Pallas kernels: 85.1 us -> 78.3 us  [per_device(): pl.pallas_call(functools.partial(kernel, n_sp, n_z), out_shape=(jax.Shape...]
where the time goes in v1:
time: 80.7 us; the launch traced here: 80.5 us
  Pallas kernels  79.9 us (99%)
    pallas_call x1, Pallas kernels, per_device(): pl.pallas_call(functools.partial(kernel, n_sp, n_z), out_shape=(jax.Shape...  78.3 us

profile of v1, /device:TPU:0, one launch (start us, length us, event | category | flops | bytes accessed | tf_op | source)
XLA Modules:
  0.0 80.5 jit_solution(16068641615847430892)
XLA Ops:
  0.6 78.3 %shard_map.104 = (bf16[2,2,32,256]{3,2,1,0:T(8,128)(2,1)}, f32[2,4,2,256]{3,2,1,0:T(2,128)}) custom-call(bf16[2,512,512]{2,1,0:T(8,128)(2,1)} %x_ref.1, f32[8,1,512]{2,1,0:T(1,128)} %bitcast.5, bf16[4096,256]{1,0:T(8,128)(2,1)} %wk_hbm.1, bf16[4096,512]{1,0:T(8,128)(2,1)} %wv_hbm.1, bf16[32,4096]{1,0:T(8,128)(2,1)} %bitcast.4, bf16[32,2048]{1,0:T(8,128)(2,1)} %up_hbm.1, ...), custom_call_target="tpu_custom_call" | custom-call | tf_op jit(solution)/shard_map/pallas_call | solution.py:895
  78.9 1.5 %shard_map.105 = (bf16[2,2,32,256]{3,2,1,0:T(8,128)(2,1)}, bf16[2,512]{1,0:T(2,128)(2,1)}) custom-call(bf16[2,2,32,256]{3,2,1,0:T(8,128)(2,1)} %get-tuple-element.4.cache_in, f32[2,4,2,256]{3,2,1,0:T(2,128)} %get-tuple-element.5.parts_ref, f32[1,256]{1,0:T(1,128)} %bitcast.7), custom_call_target="tpu_custom_call" | custom-call | tf_op jit(solution)/shard_map/pallas_call | solution.py:950

commit v2 on v1

--- a/solution.py
+++ b/solution.py
@@ -73,19 +73,17 @@
     read_send,
     read_recv,
     lent_x=None,
-    lent_wk=None,
-    lent_wv=None,
+    lent_w=None,
     lent_up=None,
     lent_bias=None,
-    lent_k=None,
-    lent_v=None,
+    lent_kv=None,
     lent_l=None,
     lent_s=None,
     lent_fade=None,
     lent_scale=None,
     hint=None,
     lent_terms=None,
-    lent_tots=None,
+    sent_tots=None,
     back_terms=None,
     back_tots=None,
     hint_send=None,
@@ -108,6 +106,7 @@
     lend = lends(n_sp, n_z, heads)
     lent = LENT_SEQ * per_seq + per_seq - 1
     tail = chunks - 1
+    relayed = min(slots, chunks // 2 + 1)
     sp = lax.axis_index("sp")
     tp = lax.axis_index("tp")
     z = tp // 2
@@ -143,9 +142,13 @@
 
     def stage_w(act):
         head = lax.rem(sp, 2)
-        for n, (src, dst, width) in enumerate(((wk_hbm, lent_wk, DK), (wv_hbm, lent_wv, DV))):
+        for n, (src, width, begin) in enumerate(((wk_hbm, DK, 0), (wv_hbm, DV, DK))):
             columns = pl.ds(pl.multiple_of(head * width, width), width)
+            dst = lent_w.at[:, begin : begin + width]
             act(pltpu.make_async_copy(src.at[:, columns], dst, load_sem.at[9 + n]))
+
+    def piece(j, zz, cc):
+        return (j * n_z + zz) * 2 + cc
 
     def chunk_rows(j):
         seq = j // per_seq
@@ -155,14 +158,14 @@
     def own_copy(j):
         seq, start = chunk_rows(j)
         return pltpu.make_async_copy(
-            x_ref.at[seq, pl.ds(start, CHUNK), :], xbuf.at[j, z, c], own_sem.at[j]
+            x_ref.at[seq, pl.ds(start, CHUNK), :], xbuf.at[piece(j, z, c)], own_sem.at[j]
         )
 
     def hop_copy(j, zz, way):
         return pltpu.make_async_remote_copy(
-            src_ref=xbuf.at[j, zz, c],
-            dst_ref=xbuf.at[j, zz, c],
-            send_sem=hop_send.at[j, zz, way],
+            src_ref=xbuf.at[piece(j, zz, c)],
+            dst_ref=xbuf.at[piece(j, zz, c)],
+            send_sem=hop_send,
             recv_sem=recv.at[j, zz, c],
             device_id={"tp": (z + 2 * way - 1) * 2 + c},
             device_id_type=MESH,
@@ -170,9 +173,9 @@
 
     def pair_copy(j, zz, cc):
         return pltpu.make_async_remote_copy(
-            src_ref=xbuf.at[j, zz, cc],
-            dst_ref=xbuf.at[j, zz, cc],
-            send_sem=pair_send.at[j, zz],
+            src_ref=xbuf.at[piece(j, zz, cc)],
+            dst_ref=xbuf.at[piece(j, zz, cc)],
+            send_sem=pair_send,
             recv_sem=recv.at[j, zz, cc],
             device_id={"tp": tp + 1 - 2 * c},
             device_id_type=MESH,
@@ -199,45 +202,55 @@
         return (j != lent) | jnp.logical_not(at_end)
 
     def lend_x(zz, act):
-        for n, peer in enumerate(peers):
+        for peer in peers:
             act(
                 pltpu.make_async_remote_copy(
-                    src_ref=xbuf.at[lent, zz, c],
+                    src_ref=xbuf.at[piece(lent, zz, c)],
                     dst_ref=lent_x.at[lax.rem(sp, 2), zz, c],
-                    send_sem=lent_x_send.at[zz, n],
-                    recv_sem=lent_x_recv.at[lax.rem(sp, 2), zz, c],
+                    send_sem=lent_x_send,
+                    recv_sem=lent_x_recv.at[lax.rem(sp, 2)],
                     device_id={"sp": peer, "tp": z * 2 + sp // 2},
                     device_id_type=MESH,
                 )
             )
 
-    def lend_w(slot, act):
+    def w_copy(slot, device, send_sem):
         rows = pl.ds(pl.multiple_of(slot * feats, feats), feats)
-        for n, both in enumerate((lent_wk, lent_wv)):
-            act(
-                pltpu.make_async_remote_copy(
-                    src_ref=both.at[rows, :],
-                    dst_ref=both.at[rows, :],
-                    send_sem=lent_w_send.at[n, slot],
-                    recv_sem=lent_w_recv.at[n, slot],
-                    device_id={"tp": inner * 2 + c},
-                    device_id_type=MESH,
-                )
-            )
-
-    def pair_w(slot, act):
-        rows = pl.ds(pl.multiple_of(slot * feats, feats), feats)
-        for n, both in enumerate((lent_wk, lent_wv)):
-            act(
-                pltpu.make_async_remote_copy(
-                    src_ref=both.at[rows, :],
-                    dst_ref=both.at[rows, :],
-                    send_sem=lent_w_pair.at[n, slot],
-                    recv_sem=lent_w_recv.at[n, slot],
-                    device_id={"tp": tp + 1 - 2 * c},
-                    device_id_type=MESH,
-                )
-            )
+        return pltpu.make_async_remote_copy(
+            src_ref=lent_w.at[rows],
+            dst_ref=lent_w.at[rows],
+            send_sem=send_sem,
+            recv_sem=lent_w_recv.at[slot],
+            device_id={"tp": device},
+            device_id_type=MESH,
+        )
+
+    def lend_w(slot):
+        return w_copy(slot, inner * 2 + c, lent_w_send)
+
+    def pair_w(slot):
+        return w_copy(slot, tp + 1 - 2 * c, lent_w_pair)
+
+    def w_copy_all(send_sem):
+        return pltpu.make_async_remote_copy(
+            src_ref=lent_w,
+            dst_ref=lent_w,
+            send_sem=send_sem,
+            recv_sem=lent_w_recv.at[0],
+            device_id={"tp": tp + 1 - 2 * c},
+            device_id_type=MESH,
+        )
+
+    def given(n):
+        both = (sent_tots, lent_terms)[n]
+        return pltpu.make_async_remote_copy(
+            src_ref=both,
+            dst_ref=both,
+            send_sem=back_send.at[n],
+            recv_sem=back_recv.at[n],
+            device_id={"tp": tp + 1 - 2 * c},
+            device_id_type=MESH,
+        )
 
     def hint_copy():
         return pltpu.make_async_remote_copy(
@@ -251,12 +264,12 @@
 
     def give_back(n, p):
         lines = pl.ds(2 * c, 2)
-        src, dst = ((lent_tots, back_tots), (lent_terms.at[p], back_terms))[n]
+        src, dst = ((sent_tots.at[p], back_tots), (lent_terms.at[p], back_terms))[n]
         return pltpu.make_async_remote_copy(
             src_ref=src,
             dst_ref=dst.at[lax.rem(sp, 2), lines],
-            send_sem=back_send.at[n, p],
-            recv_sem=back_recv.at[n, lax.rem(sp, 2), c],
+            send_sem=back_send.at[n],
+            recv_sem=back_recv.at[n],
             device_id={"sp": p, "tp": end * 2 + sp // 2},
             device_id_type=MESH,
         )
@@ -307,8 +320,7 @@
 
         @pl.when(at_inner)
         def _():
-            lent_k[...] = jnp.zeros_like(lent_k)
-            lent_v[...] = jnp.zeros_like(lent_v)
+            lent_kv[...] = jnp.zeros_like(lent_kv)
             lent_l[...] = jnp.zeros_like(lent_l)
             lent_s[...] = jnp.zeros_like(lent_s)
 
@@ -359,7 +371,7 @@
 
     def add_shard(j, zz, cc):
         slot = zz * 2 + cc
-        wide = xbuf[j, zz, cc].astype(F32)
+        wide = xbuf[piece(j, zz, cc)].astype(F32)
         scaled = (wide * gain_ref[slot]).astype(BF16)
         project(scaled, slot, j, (wk, wv), (acc_k, acc_v))
         reduce_rank(wide, scaled, slot, j, acc_l, acc_s)
@@ -472,40 +484,59 @@
         def _():
             send_terms(seq)
 
-    def tot_copy(seq, peer, slot):
+    def tot_copy(seq, peer):
         return pltpu.make_async_remote_copy(
             src_ref=tots.at[seq, sp],
-            dst_ref=tots.at[seq, slot],
-            send_sem=tot_send.at[seq, peer],
-            recv_sem=tot_recv.at[seq, slot],
+            dst_ref=tots.at[seq, sp],
+            send_sem=tot_send.at[seq],
+            recv_sem=tot_recv.at[seq],
             device_id={"sp": peer},
             device_id_type=MESH,
         )
 
-    def term_copy(seq, peer, slot):
+    def term_copy(seq, peer):
         return pltpu.make_async_remote_copy(
             src_ref=terms.at[seq, peer],
-            dst_ref=landed.at[seq, slot],
-            send_sem=term_send.at[seq, peer],
-            recv_sem=term_recv.at[seq, slot],
+            dst_ref=landed.at[seq, sp],
+            send_sem=term_send.at[seq],
+            recv_sem=term_recv.at[seq],
             device_id={"sp": peer},
             device_id_type=MESH,
         )
 
-    def read_copy(seq, peer, slot):
+    def read_copy(seq, peer):
         return pltpu.make_async_remote_copy(
             src_ref=reads.at[seq, sp],
-            dst_ref=reads.at[seq, slot],
-            send_sem=read_send.at[seq, peer],
-            recv_sem=read_recv.at[seq, slot],
+            dst_ref=reads.at[seq, sp],
+            send_sem=read_send.at[seq],
+            recv_sem=read_recv.at[seq],
             device_id={"sp": peer},
             device_id_type=MESH,
         )
+
+    def others(ref, seq, sems):
+        return pltpu.make_async_remote_copy(
+            src_ref=ref.at[seq, pl.ds(0, n_sp - 1)],
+            dst_ref=ref.at[seq, pl.ds(0, n_sp - 1)],
+            send_sem=sems[0].at[seq],
+            recv_sem=sems[1].at[seq],
+            device_id={"sp": peers[0]},
+            device_id_type=MESH,
+        )
+
+    def all_tots(seq):
+        return others(tots, seq, (tot_send, tot_recv))
+
+    def all_terms(seq):
+        return others(landed, seq, (term_send, term_recv))
+
+    def all_reads(seq):
+        return others(reads, seq, (read_send, read_recv))
 
     def send_total(seq):
         tots[seq, sp] = carry[...]
         for peer in peers:
-            tot_copy(seq, peer, sp).start()
+            tot_copy(seq, peer).start()
 
     def send_terms(seq):
         for h in range(heads):
@@ -513,21 +544,18 @@
                 row = h * DK + p * share
                 terms[seq, p, h] = state[seq, row : row + share, :].astype(BF16)
         for peer in peers:
-            term_copy(seq, peer, sp).start()
-
-    def await_back(n):
+            term_copy(seq, peer).start()
+
+    def back_copy(n):
         both = (back_tots, back_terms)[n]
-        for head in range(heads):
-            for core in range(2):
-                lines = pl.ds(2 * core, 2)
-                pltpu.make_async_remote_copy(
-                    src_ref=both.at[head, lines],
-                    dst_ref=both.at[head, lines],
-                    send_sem=back_send.at[n, 0],
-                    recv_sem=back_recv.at[n, head, core],
-                    device_id={"tp": inner * 2 + c},
-                    device_id_type=MESH,
-                ).wait_recv()
+        return pltpu.make_async_remote_copy(
+            src_ref=both,
+            dst_ref=both,
+            send_sem=back_send.at[n],
+            recv_sem=back_recv.at[n],
+            device_id={"tp": inner * 2 + c},
+            device_id_type=MESH,
+        )
 
     def column(row, begin, size):
         chosen = (
@@ -540,8 +568,7 @@
         return query_ref[seq : seq + 1, h * DK : (h + 1) * DK].astype(F32)
 
     def send_parts(seq):
-        for peer in peers:
-            tot_copy(seq, peer, peer).wait_recv()
+        all_tots(seq).wait_recv()
         for h in range(heads):
             after = jnp.zeros((1, DK), F32)
             for p in range(n_sp):
@@ -552,11 +579,11 @@
                 asked * state[seq, h * DK : (h + 1) * DK, :], axis=0, keepdims=True
             )
         for peer in peers:
-            read_copy(seq, peer, sp).start()
+            read_copy(seq, peer).start()
 
     def sum_terms(seq, loaned):
         if loaned:
-            pl.when(at_end)(lambda: await_back(0))
+            pl.when(at_end)(lambda: back_copy(0).wait_recv())
         after = [jnp.zeros((1, DK), F32)] * heads
         factors = [None] * n_sp
         back_factors = [None] * n_sp
@@ -566,10 +593,9 @@
             if loaned:
                 back_factors[p] = [column(jnp.exp(row), sp * share, share) for row in after]
                 after = [after[h] + back_tots[h, p] for h in range(heads)]
-        for peer in peers:
-            term_copy(seq, peer, peer).wait_recv()
+        all_terms(seq).wait_recv()
         if loaned:
-            pl.when(at_end)(lambda: await_back(1))
+            pl.when(at_end)(lambda: back_copy(1).wait_recv())
         for h in range(heads):
             own = state[seq, pl.ds(pl.multiple_of(h * DK + sp * share, share), share), :]
             total = jnp.zeros((share, DV), F32)
@@ -581,8 +607,7 @@
             cache_ref[seq, h] = total.astype(BF16)
 
     def send_reads(seq):
-        for peer in peers:
-            tot_copy(seq, peer, peer).wait_recv()
+        all_tots(seq).wait_recv()
         sum_terms(seq, True)
         for h in range(heads):
             reads[seq, sp, h : h + 1, :] = jnp.sum(
@@ -591,11 +616,10 @@
                 keepdims=True,
             )
         for peer in peers:
-            read_copy(seq, peer, sp).start()
+            read_copy(seq, peer).start()
 
     def give_read(seq):
-        for peer in peers:
-            read_copy(seq, peer, peer).wait_recv()
+        all_reads(seq).wait_recv()
         parts_ref[seq] = reads[seq]
 
     def lent_scaled(slot):
@@ -608,26 +632,27 @@
         def collect(slot, _):
             zz, cc = slot // 2, lax.rem(slot, 2)
             for line in range(2):
-                mine = 2 * c + line == sp
-
-                @pl.when(mine)
+
+                @pl.when(2 * c + line == sp)
                 def _():
-                    lent_x[line, zz, cc] = xbuf[lent, zz, cc]
-
-                @pl.when(jnp.logical_not(mine))
-                def _():
-                    pltpu.make_async_remote_copy(
-                        src_ref=lent_x.at[line, zz, cc],
-                        dst_ref=lent_x.at[line, zz, cc],
-                        send_sem=lent_x_send.at[zz, 0],
-                        recv_sem=lent_x_recv.at[line, zz, cc],
-                        device_id={"tp": tp + 1 - 2 * c},
-                        device_id_type=MESH,
-                    ).wait_recv()
+                    lent_x[line, zz, cc] = xbuf[piece(lent, zz, cc)]
 
             wide, scaled = lent_scaled(slot)
             reduce_rank(wide, scaled, slot, every, lent_l, lent_s)
             return 0
+
+        for line in range(2):
+
+            @pl.when(2 * c + line != sp)
+            def _():
+                pltpu.make_async_remote_copy(
+                    src_ref=lent_x.at[line],
+                    dst_ref=lent_x.at[line],
+                    send_sem=lent_x_send,
+                    recv_sem=lent_x_recv.at[line],
+                    device_id={"tp": tp + 1 - 2 * c},
+                    device_id_type=MESH,
+                ).wait_recv()
 
         lax.fori_loop(0, slots, collect, 0)
         blocks = [slice(line * CHUNK, (line + 1) * CHUNK) for line in range(2)]
@@ -636,27 +661,31 @@
             weights, total = faded(low_rank, lent_up, lent_bias, jnp.zeros((1, DK), F32))
             lent_fade[rows] = weights
             lent_scale[rows] = jnp.broadcast_to(inv_rms, weights.shape)
-            lent_tots[line] = total
+            for q in range(n_sp):
+                sent_tots[q, line] = total
         for p in range(n_sp):
             give_back(0, p).start()
+        send_reads(LENT_SEQ)
 
         def multiply(slot, _):
-            pair_w(slot, lambda copy: copy.wait_recv())
-
-            @pl.when(c == sp // 2)
-            def _():
-                pair_w(slot, lambda copy: copy.start())
+            @pl.when((c != sp // 2) | (slot >= relayed))
+            def _():
+                pair_w(slot).wait_recv()
+
+            @pl.when((c == sp // 2) & (slot >= relayed))
+            def _():
+                pair_w(slot).start()
 
             _, scaled = lent_scaled(slot)
-            project(scaled, slot, every, (lent_wk, lent_wv), (lent_k, lent_v))
+            project(scaled, slot, every, (lent_w,), (lent_kv,))
             return 0
 
         lax.fori_loop(0, slots, multiply, 0)
         for line, rows in enumerate(blocks):
             inv_rms = lent_scale[rows, :1]
-            keys = (lent_k[rows] * inv_rms).astype(BF16).astype(F32)
+            keys = (lent_kv[rows, :DK] * inv_rms).astype(BF16).astype(F32)
             weighted = keys * lent_fade[rows]
-            values = (lent_v[rows] * inv_rms).astype(BF16)
+            values = (lent_kv[rows, DK:] * inv_rms).astype(BF16)
             block = jnp.dot(weighted.T.astype(BF16), values, preferred_element_type=F32)
             for p in range(n_sp):
                 lent_terms[p, line] = block[p * share : (p + 1) * share].astype(BF16)
@@ -738,10 +767,18 @@
                 settle(last_i, last_j)
                 take_hint()
 
+            due = (2 * j + 1) // 3
+            relaying = at_inner & (c == sp // 2) & (i == final_step) & ((3 * due + 1) // 2 == j)
+
+            @pl.when(relaying & (due < relayed))
+            def _():
+                pair_w(due).wait_recv()
+                pair_w(due).start()
+
             @pl.when(lender & (t == 2 * chunks))
             def _():
                 def lend_slot(slot, _):
-                    lend_w(slot, lambda copy: copy.start())
+                    lend_w(slot).start()
                     return 0
 
                 lax.fori_loop(0, slots, lend_slot, 0)
@@ -763,7 +800,6 @@
 
         @pl.when(at_inner)
         def _():
-            send_reads(LENT_SEQ)
             work_off()
 
     rest = [seq for seq in range(seqs) if not (lend and seq == LENT_SEQ)]
@@ -774,56 +810,47 @@
     for seq in rest:
         sum_terms(seq, False)
 
-    def drain(i, _):
-        zz = source(i)
-
-        @pl.when((zz >= 0) & (zz < n_z))
-        def _():
-            def inside(j, _):
-                @pl.when((i == 0) | used(j))
-                def _():
-                    each_way(j, zz, lambda copy: copy.wait_send())
-
-                @pl.when(used(j))
-                def _():
-                    pair_copy(j, zz, c).wait_send()
-
-                return 0
-
-            lax.fori_loop(0, chunks, inside, 0)
-
-        return 0
-
-    lax.fori_loop(0, 2 * n_z - 2, drain, 0)
+    def drained(count, send_sem):
+        pltpu.make_async_remote_copy(
+            src_ref=xbuf.at[pl.ds(0, count)],
+            dst_ref=xbuf.at[pl.ds(0, count)],
+            send_sem=send_sem,
+            recv_sem=recv.at[0, 0, 0],
+            device_id={"tp": tp + 1 - 2 * c},
+            device_id_type=MESH,
+        ).wait_send()
+
+    for plane in range(n_z):
+        edge = plane in (0, n_z - 1)
+        hops = (0 if plane == 0 else n_z - plane) + (0 if plane == n_z - 1 else plane + 1)
+        hops = hops * chunks
+        pairs = n_z * chunks
+        if lend and plane in (1, n_z - 2):
+            hops -= n_z - 1
+        if lend and edge:
+            pairs -= n_z
+
+        @pl.when(z == plane)
+        def _():
+            drained(hops, hop_send)
+            drained(pairs, pair_send)
+
     if lend:
-
-        def drain_slot(slot, _):
-            pl.when(lender)(lambda: lend_w(slot, lambda copy: copy.wait_send()))
-
-            @pl.when(at_inner & (c == sp // 2))
-            def _():
-                pair_w(slot, lambda copy: copy.wait_send())
-
-            return 0
-
-        lax.fori_loop(0, slots, drain_slot, 0)
+        pl.when(lender)(lambda: w_copy_all(lent_w_send).wait_send())
 
         @pl.when(at_inner)
         def _():
-            for zz in range(n_z):
-                lend_x(zz, lambda copy: copy.wait_send())
-            for p in range(n_sp):
-                give_back(0, p).wait_send()
-                give_back(1, p).wait_send()
+            pl.when(c == sp // 2)(lambda: w_copy_all(lent_w_pair).wait_send())
+            drained(n_z * (n_sp - 1), lent_x_send)
+            given(0).wait_send()
+            given(1).wait_send()
             hint_copy().wait_send()
 
     for seq in range(seqs):
         give_read(seq)
     for seq in range(seqs):
-        for peer in peers:
-            tot_copy(seq, peer, sp).wait_send()
-            term_copy(seq, peer, sp).wait_send()
-            read_copy(seq, peer, sp).wait_send()
+        for kind in (all_tots, all_terms, all_reads):
+            kind(seq).wait_send()
 
 
 def norm_kernel(cache_in, parts_ref, gain_ref, cache_ref, read_ref):
@@ -867,30 +894,28 @@
     if lends(n_sp, n_z, heads):
         lent = [
             pltpu.VMEM((2, n_z, 2, CHUNK, feats), BF16),
-            pltpu.VMEM((model, DK), BF16),
-            pltpu.VMEM((model, DV), BF16),
+            pltpu.VMEM((model, DK + DV), BF16),
             pltpu.VMEM((rank, DK), BF16),
             pltpu.VMEM((1, DK), F32),
-            pltpu.VMEM((2 * CHUNK, DK), F32),
-            pltpu.VMEM((2 * CHUNK, DV), F32),
+            pltpu.VMEM((2 * CHUNK, DK + DV), F32),
             pltpu.VMEM((2 * CHUNK, rank), F32),
             pltpu.VMEM((2 * CHUNK, 128), F32),
             pltpu.VMEM((2 * CHUNK, DK), F32),
             pltpu.VMEM((2 * CHUNK, DK), F32),
             pltpu.VMEM((rank + 8, CHUNK), F32),
             pltpu.VMEM((n_sp, 2, share, DV), BF16),
-            pltpu.VMEM((2, 1, DK), F32),
+            pltpu.VMEM((n_sp, 2, 1, DK), F32),
             pltpu.VMEM((heads, n_sp, share, DV), BF16),
             pltpu.VMEM((heads, n_sp, 1, DK), F32),
             dma,
             dma,
-            dma((n_z, n_sp - 1)),
-            dma((2, n_z, 2)),
-            dma((2, slots)),
-            dma((2, slots)),
-            dma((2, slots)),
-            dma((2, n_sp)),
-            dma((2, heads, 2)),
+            dma,
+            dma((2,)),
+            dma,
+            dma,
+            dma((slots,)),
+            dma((2,)),
+            dma((2,)),
         ]
     cache, parts = pl.pallas_call(
         functools.partial(kernel, n_sp, n_z),
@@ -901,7 +926,7 @@
         in_specs=[hbm] * 8,
         out_specs=(vmem, vmem),
         scratch_shapes=[
-            pltpu.VMEM((chunks, n_z, 2, CHUNK, feats), BF16),
+            pltpu.VMEM((chunks * slots, CHUNK, feats), BF16),
             pltpu.VMEM((model, key_cols), BF16),
             pltpu.VMEM((model, value_cols), BF16),
             pltpu.VMEM((rank, model), BF16),
@@ -923,15 +948,15 @@
             pltpu.VMEM((seqs, n_sp, heads, DV), F32),
             dma((11,)),
             dma((chunks,)),
+            dma,
+            dma,
             dma((chunks, n_z, 2)),
-            dma((chunks, n_z)),
-            dma((chunks, n_z, 2)),
-            dma((seqs, n_sp)),
-            dma((seqs, n_sp)),
-            dma((seqs, n_sp)),
-            dma((seqs, n_sp)),
-            dma((seqs, n_sp)),
-            dma((seqs, n_sp)),
+            dma((seqs,)),
+            dma((seqs,)),
+            dma((seqs,)),
+            dma((seqs,)),
+            dma((seqs,)),
+            dma((seqs,)),
         ]
         + lent,
         compiler_params=pltpu.CompilerParams(

time: 80.7 us -> 78.5 us (0.973)
  Pallas kernels: 79.9 us -> 77.7 us
    pallas_call x1, Pallas kernels: 78.3 us -> 76.2 us  [per_device(): pl.pallas_call(functools.partial(kernel, n_sp, n_z), out_shape=(jax.Shape...]
where the time goes in v2:
time: 78.5 us; the launch traced here: 78.4 us
  Pallas kernels  77.7 us (99%)
    pallas_call x1, Pallas kernels, per_device(): pl.pallas_call(functools.partial(kernel, n_sp, n_z), out_shape=(jax.Shape...  76.2 us

profile of v2, /device:TPU:0, one launch (start us, length us, event | category | flops | bytes accessed | tf_op | source)
XLA Modules:
  0.0 78.4 jit_solution(11966244092670718063)
XLA Ops:
  0.6 76.2 %shard_map.104 = (bf16[2,2,32,256]{3,2,1,0:T(8,128)(2,1)}, f32[2,4,2,256]{3,2,1,0:T(2,128)}) custom-call(bf16[2,512,512]{2,1,0:T(8,128)(2,1)} %x_ref.1, f32[8,1,512]{2,1,0:T(1,128)} %bitcast.5, bf16[4096,256]{1,0:T(8,128)(2,1)} %wk_hbm.1, bf16[4096,512]{1,0:T(8,128)(2,1)} %wv_hbm.1, bf16[32,4096]{1,0:T(8,128)(2,1)} %bitcast.4, bf16[32,2048]{1,0:T(8,128)(2,1)} %up_hbm.1, ...), custom_call_target="tpu_custom_call" | custom-call | tf_op jit(solution)/shard_map/pallas_call | solution.py:920
  76.8 1.5 %shard_map.105 = (bf16[2,2,32,256]{3,2,1,0:T(8,128)(2,1)}, bf16[2,512]{1,0:T(2,128)(2,1)}) custom-call(bf16[2,2,32,256]{3,2,1,0:T(8,128)(2,1)} %get-tuple-element.4.cache_in, f32[2,4,2,256]{3,2,1,0:T(2,128)} %get-tuple-element.5.parts_ref, f32[1,256]{1,0:T(1,128)} %bitcast.7), custom_call_target="tpu_custom_call" | custom-call | tf_op jit(solution)/shard_map/pallas_call | solution.py:975

commit v3 on v2

--- a/solution.py
+++ b/solution.py
@@ -11,6 +11,7 @@
 DV = 256
 CHUNK = 128
 LENT_SEQ = 0
+EXTRA = 64
 MESH = pl.DeviceIdType.MESH
 F32 = jnp.float32
 BF16 = jnp.bfloat16
@@ -86,6 +87,13 @@
     sent_tots=None,
     back_terms=None,
     back_tots=None,
+    asks=None,
+    asked=None,
+    sent_reads=None,
+    back_reads=None,
+    lent_state=None,
+    ask_send=None,
+    ask_recv=None,
     hint_send=None,
     hint_recv=None,
     lent_x_send=None,
@@ -106,7 +114,9 @@
     lend = lends(n_sp, n_z, heads)
     lent = LENT_SEQ * per_seq + per_seq - 1
     tail = chunks - 1
-    relayed = min(slots, chunks // 2 + 1)
+    split = lent - 1
+    lent_rows = CHUNK + EXTRA
+    relayed = min(slots - 2, chunks // 2 + 1)
     sp = lax.axis_index("sp")
     tp = lax.axis_index("tp")
     z = tp // 2
@@ -117,6 +127,7 @@
     end = jnp.where(low_half, 0, n_z - 1)
     inner = jnp.where(low_half, 1, n_z - 2)
     at_inner = z == inner
+    far_end = n_z - 1 - end
     flip = jnp.where(low_half, 1, -1)
     reach = jnp.where(low_half, n_z - 1 - z, z)
     final_step = 2 * reach - 1
@@ -147,8 +158,13 @@
             dst = lent_w.at[:, begin : begin + width]
             act(pltpu.make_async_copy(src.at[:, columns], dst, load_sem.at[9 + n]))
 
-    def piece(j, zz, cc):
-        return (j * n_z + zz) * 2 + cc
+    def piece(j, zz, cc, skip=0):
+        start = ((j * n_z + zz) * 2 + cc) * CHUNK + skip
+        return pl.ds(pl.multiple_of(start, 16), CHUNK - skip)
+
+    def opening(zz, cc):
+        start = ((split * n_z + zz) * 2 + cc) * CHUNK
+        return pl.ds(pl.multiple_of(start, 16), EXTRA)
 
     def chunk_rows(j):
         seq = j // per_seq
@@ -161,25 +177,33 @@
             x_ref.at[seq, pl.ds(start, CHUNK), :], xbuf.at[piece(j, z, c)], own_sem.at[j]
         )
 
-    def hop_copy(j, zz, way):
-        return pltpu.make_async_remote_copy(
-            src_ref=xbuf.at[piece(j, zz, c)],
-            dst_ref=xbuf.at[piece(j, zz, c)],
+    def hop_copy(j, zz, way, skip=0):
+        return pltpu.make_async_remote_copy(
+            src_ref=xbuf.at[piece(j, zz, c, skip)],
+            dst_ref=xbuf.at[piece(j, zz, c, skip)],
             send_sem=hop_send,
             recv_sem=recv.at[j, zz, c],
             device_id={"tp": (z + 2 * way - 1) * 2 + c},
             device_id_type=MESH,
         )
 
-    def pair_copy(j, zz, cc):
-        return pltpu.make_async_remote_copy(
-            src_ref=xbuf.at[piece(j, zz, cc)],
-            dst_ref=xbuf.at[piece(j, zz, cc)],
+    def pair_copy(j, zz, cc, skip=0):
+        return pltpu.make_async_remote_copy(
+            src_ref=xbuf.at[piece(j, zz, cc, skip)],
+            dst_ref=xbuf.at[piece(j, zz, cc, skip)],
             send_sem=pair_send,
             recv_sem=recv.at[j, zz, cc],
             device_id={"tp": tp + 1 - 2 * c},
             device_id_type=MESH,
         )
+
+    def each_pair(j, zz, cc, act):
+        if not lend:
+            act(pair_copy(j, zz, cc))
+            return
+        short = at_end & (j == split)
+        pl.when(short)(lambda: act(pair_copy(j, zz, cc, EXTRA)))
+        pl.when(jnp.logical_not(short))(lambda: act(pair_copy(j, zz, cc)))
 
     def each_way(j, zz, act):
         for way, edge in ((0, 0), (1, n_z - 1)):
@@ -187,32 +211,37 @@
             beyond = (zz >= z) if way == 0 else (zz <= z)
             wanted = (z != edge) & beyond
             if lend:
-                wanted = wanted & ((j != lent) | (there != edge))
-
-            @pl.when(wanted)
-            def _():
-                act(hop_copy(j, zz, way))
+                short = (j == split) & (there == edge)
+                pl.when(wanted & short)(lambda: act(hop_copy(j, zz, way, EXTRA)))
+                wanted = wanted & jnp.logical_not(short) & ((j != lent) | (there != edge))
+            pl.when(wanted)(lambda: act(hop_copy(j, zz, way)))
 
     def held(j, zz):
-        return at_inner & (j == tail) & (flip * (zz - z) > 0)
+        return at_inner & (j == tail) & (zz == far_end)
 
     def used(j):
         if not lend:
             return j >= 0
         return (j != lent) | jnp.logical_not(at_end)
 
-    def lend_x(zz, act):
+    def lend_x(j, zz):
         for peer in peers:
-            act(
-                pltpu.make_async_remote_copy(
-                    src_ref=xbuf.at[piece(lent, zz, c)],
-                    dst_ref=lent_x.at[lax.rem(sp, 2), zz, c],
-                    send_sem=lent_x_send,
-                    recv_sem=lent_x_recv.at[lax.rem(sp, 2)],
-                    device_id={"sp": peer, "tp": z * 2 + sp // 2},
-                    device_id_type=MESH,
-                )
-            )
+            for whole in (True, False):
+
+                @pl.when(j == (lent if whole else split))
+                def _():
+                    begin, size = (0, CHUNK) if whole else (CHUNK, EXTRA)
+                    rows = piece(lent, zz, c) if whole else opening(zz, c)
+                    pltpu.make_async_remote_copy(
+                        src_ref=xbuf.at[rows],
+                        dst_ref=lent_x.at[lax.rem(sp, 2), zz, c, pl.ds(begin, size)],
+                        send_sem=lent_x_send,
+                        recv_sem=lent_x_recv.at[
+                            lax.rem(sp, 2), jnp.where(zz == far_end, 1, 0)
+                        ],
+                        device_id={"sp": peer, "tp": z * 2 + sp // 2},
+                        device_id_type=MESH,
+                    ).start()
 
     def w_copy(slot, device, send_sem):
         rows = pl.ds(pl.multiple_of(slot * feats, feats), feats)
@@ -242,7 +271,7 @@
         )
 
     def given(n):
-        both = (sent_tots, lent_terms)[n]
+        both = (sent_tots, lent_terms, sent_reads)[n]
         return pltpu.make_async_remote_copy(
             src_ref=both,
             dst_ref=both,
@@ -252,6 +281,16 @@
             device_id_type=MESH,
         )
 
+    def ask_copy(core):
+        return pltpu.make_async_remote_copy(
+            src_ref=asks.at[pl.ds(2 * core, 2)],
+            dst_ref=asked,
+            send_sem=ask_send,
+            recv_sem=ask_recv,
+            device_id={"tp": inner * 2 + core},
+            device_id_type=MESH,
+        )
+
     def hint_copy():
         return pltpu.make_async_remote_copy(
             src_ref=hint,
@@ -264,10 +303,14 @@
 
     def give_back(n, p):
         lines = pl.ds(2 * c, 2)
-        src, dst = ((sent_tots.at[p], back_tots), (lent_terms.at[p], back_terms))[n]
+        src, dst = (
+            (sent_tots.at[p], back_tots.at[lax.rem(sp, 2), lines]),
+            (lent_terms.at[p], back_terms.at[lax.rem(sp, 2), lines]),
+            (sent_reads.at[p], back_reads.at[lax.rem(sp, 2), c]),
+        )[n]
         return pltpu.make_async_remote_copy(
             src_ref=src,
-            dst_ref=dst.at[lax.rem(sp, 2), lines],
+            dst_ref=dst,
             send_sem=back_send.at[n],
             recv_sem=back_recv.at[n],
             device_id={"sp": p, "tp": end * 2 + sp // 2},
@@ -328,6 +371,7 @@
         def _():
             back_terms[...] = jnp.zeros_like(back_terms)
             back_tots[...] = jnp.zeros_like(back_tots)
+            back_reads[...] = jnp.zeros_like(back_reads)
 
     pl.semaphore_wait(barrier, far)
 
@@ -337,7 +381,7 @@
 
         @pl.when(used(j))
         def _():
-            pair_copy(j, z, c).start()
+            each_pair(j, z, c, lambda copy: copy.start())
 
         return 0
 
@@ -346,7 +390,8 @@
 
         @pl.when(at_inner)
         def _():
-            lend_x(z, lambda copy: copy.start())
+            lend_x(split, z)
+            lend_x(lent, z)
 
     for load in loads:
         load.wait()
@@ -369,9 +414,15 @@
             total = total + square[:, lane : lane + 128]
         acc_square[rows] += total
 
+    def skipped(j):
+        return jnp.where(at_end & (j == split), EXTRA, 0)
+
     def add_shard(j, zz, cc):
         slot = zz * 2 + cc
         wide = xbuf[piece(j, zz, cc)].astype(F32)
+        if lend:
+            row = lax.broadcasted_iota(jnp.int32, wide.shape, 0)
+            wide = jnp.where(row >= skipped(j), wide, 0.0)
         scaled = (wide * gain_ref[slot]).astype(BF16)
         project(scaled, slot, j, (wk, wv), (acc_k, acc_v))
         reduce_rank(wide, scaled, slot, j, acc_l, acc_s)
@@ -387,7 +438,7 @@
         def _():
             @pl.when(i > 0)
             def _():
-                pair_copy(j, zz, c).wait_recv()
+                each_pair(j, zz, c, lambda copy: copy.wait_recv())
                 if lend:
 
                     @pl.when(jnp.logical_not(held(j, zz)))
@@ -396,12 +447,10 @@
 
                 else:
                     each_way(j, zz, lambda copy: copy.start())
-                pair_copy(j, zz, c).start()
+                each_pair(j, zz, c, lambda copy: copy.start())
                 if lend:
 
-                    @pl.when(at_inner & (j == lent))
-                    def _():
-                        lend_x(zz, lambda copy: copy.start())
+                    pl.when(at_inner)(lambda: lend_x(j, zz))
 
             add_shard(j, zz, c)
 
@@ -410,23 +459,27 @@
 
         @pl.when(used(j))
         def _():
-            pair_copy(j, zz, 1 - c).wait_recv()
+            each_pair(j, zz, 1 - c, lambda copy: copy.wait_recv())
             add_shard(j, zz, 1 - c)
 
     def normed(acc_rank, acc_square, rows):
         inv_rms = lax.rsqrt(jnp.sum(acc_square[rows], axis=1, keepdims=True) / model + 1e-06)
         return acc_rank[rows] * inv_rms, inv_rms
 
-    def faded(low_rank, gate_up, gate_bias, start):
+    def faded(low_rank, gate_up, gate_bias, start, skip=None):
+        size = low_rank.shape[0]
         gate = gate_bias[...] + jnp.dot(
             jnp.concatenate(split3(low_rank), axis=1),
             jnp.concatenate([gate_up[...]] * 3, axis=0),
             preferred_element_type=F32,
         )
         log_decay = (jnp.minimum(gate, 0.0) - jnp.log1p(jnp.exp(-jnp.abs(gate)))) / 16.0
+        if skip is not None:
+            row = lax.broadcasted_iota(jnp.int32, log_decay.shape, 0)
+            log_decay = jnp.where(row >= skip, log_decay, 0.0)
         later = (
-            lax.broadcasted_iota(jnp.int32, (CHUNK, CHUNK), 1)
-            > lax.broadcasted_iota(jnp.int32, (CHUNK, CHUNK), 0)
+            lax.broadcasted_iota(jnp.int32, (size, size), 1)
+            > lax.broadcasted_iota(jnp.int32, (size, size), 0)
         ).astype(BF16)
         suffix = start + jnp.dot(
             jnp.concatenate([later] * 3, axis=1),
@@ -436,7 +489,8 @@
         return jnp.exp(suffix), start + jnp.sum(log_decay, axis=0, keepdims=True)
 
     def fade_chunk(j, low_rank, inv_rms):
-        weights, total = faded(low_rank, up, bias, carry[...])
+        skip = skipped(j) if lend else None
+        weights, total = faded(low_rank, up, bias, carry[...], skip)
         fade[...] = weights
         scale[...] = jnp.broadcast_to(inv_rms, scale.shape)
         carry[...] = total
@@ -547,7 +601,7 @@
             term_copy(seq, peer).start()
 
     def back_copy(n):
-        both = (back_tots, back_terms)[n]
+        both = (back_tots, back_terms, back_reads)[n]
         return pltpu.make_async_remote_copy(
             src_ref=both,
             dst_ref=both,
@@ -568,22 +622,49 @@
         return query_ref[seq : seq + 1, h * DK : (h + 1) * DK].astype(F32)
 
     def send_parts(seq):
-        all_tots(seq).wait_recv()
+        loaned = lend and seq == LENT_SEQ
+        if loaned:
+            pl.when(jnp.logical_not(at_end))(lambda: all_tots(seq).wait_recv())
+        else:
+            all_tots(seq).wait_recv()
         for h in range(heads):
             after = jnp.zeros((1, DK), F32)
             for p in range(n_sp):
                 total = tots[seq, p][:, h * DK : (h + 1) * DK]
+                if loaned:
+                    total = total + back_tots[h, p]
                 after = after + jnp.where(p > sp, total, 0.0)
-            asked = column(query(seq, h) * jnp.exp(after), 0, DK)
+            wanted = column(query(seq, h) * jnp.exp(after), 0, DK)
             reads[seq, sp, h : h + 1, :] = jnp.sum(
-                asked * state[seq, h * DK : (h + 1) * DK, :], axis=0, keepdims=True
+                wanted * state[seq, h * DK : (h + 1) * DK, :], axis=0, keepdims=True
             )
         for peer in peers:
             read_copy(seq, peer).start()
 
+    def send_asks():
+        all_tots(LENT_SEQ).wait_recv()
+        back_copy(0).wait_recv()
+
+        def chosen(rows):
+            picked = rows[0]
+            for h in range(1, heads):
+                picked = jnp.where(lax.rem(sp, 2) == h, rows[h], picked)
+            return picked
+
+        after = jnp.zeros((1, DK), F32)
+        asker = chosen([query(LENT_SEQ, h) for h in range(heads)])
+        for p in reversed(range(n_sp)):
+            kept = [tots[LENT_SEQ, p][:, h * DK : (h + 1) * DK] for h in range(heads)]
+            after = after + chosen(kept)
+            asks[p] = asker * jnp.exp(after)
+            after = after + chosen([back_tots[h, p] for h in range(heads)])
+
+        @pl.when(lender)
+        def _():
+            for core in range(2):
+                ask_copy(core).start()
+
     def sum_terms(seq, loaned):
-        if loaned:
-            pl.when(at_end)(lambda: back_copy(0).wait_recv())
         after = [jnp.zeros((1, DK), F32)] * heads
         factors = [None] * n_sp
         back_factors = [None] * n_sp
@@ -606,57 +687,61 @@
                     total = total + back_factors[p][h] * back_terms[h, p].astype(F32)
             cache_ref[seq, h] = total.astype(BF16)
 
-    def send_reads(seq):
-        all_tots(seq).wait_recv()
-        sum_terms(seq, True)
-        for h in range(heads):
-            reads[seq, sp, h : h + 1, :] = jnp.sum(
-                column(query(seq, h), sp * share, share) * cache_ref[seq, h].astype(F32),
-                axis=0,
-                keepdims=True,
-            )
-        for peer in peers:
-            read_copy(seq, peer).start()
-
     def give_read(seq):
         all_reads(seq).wait_recv()
         parts_ref[seq] = reads[seq]
+        if lend and seq == LENT_SEQ:
+            pl.when(at_end)(lambda: back_copy(2).wait_recv())
+            for h in range(heads):
+                parts_ref[seq, 0, h : h + 1] = (
+                    reads[seq, 0, h : h + 1] + back_reads[h, 0] + back_reads[h, 1]
+                )
 
     def lent_scaled(slot):
-        wide = lent_x[:, slot // 2, lax.rem(slot, 2)].reshape(2 * CHUNK, feats).astype(F32)
+        wide = lent_x[:, slot // 2, lax.rem(slot, 2)].reshape(2 * lent_rows, feats).astype(F32)
         return wide, (wide * gain_ref[slot]).astype(BF16)
 
-    def work_off():
-        every = slice(None)
-
-        def collect(slot, _):
-            zz, cc = slot // 2, lax.rem(slot, 2)
-            for line in range(2):
-
-                @pl.when(2 * c + line == sp)
-                def _():
-                    lent_x[line, zz, cc] = xbuf[piece(lent, zz, cc)]
-
-            wide, scaled = lent_scaled(slot)
-            reduce_rank(wide, scaled, slot, every, lent_l, lent_s)
-            return 0
-
+    lent_blocks = [slice(line * lent_rows, (line + 1) * lent_rows) for line in range(2)]
+    every = slice(None)
+
+    def collect(slot, _):
+        zz, cc = slot // 2, lax.rem(slot, 2)
+        for line in range(2):
+
+            @pl.when(2 * c + line == sp)
+            def _():
+                lent_x[line, zz, cc, :CHUNK] = xbuf[piece(lent, zz, cc)]
+                lent_x[line, zz, cc, CHUNK:] = xbuf[opening(zz, cc)]
+
+        wide, scaled = lent_scaled(slot)
+        reduce_rank(wide, scaled, slot, every, lent_l, lent_s)
+        return 0
+
+    def await_lent(far):
+        begin, size = (far_end, 1) if far else (jnp.where(low_half, 0, 1), n_z - 1)
         for line in range(2):
 
             @pl.when(2 * c + line != sp)
             def _():
                 pltpu.make_async_remote_copy(
-                    src_ref=lent_x.at[line],
-                    dst_ref=lent_x.at[line],
+                    src_ref=lent_x.at[line, pl.ds(begin, size)],
+                    dst_ref=lent_x.at[line, pl.ds(begin, size)],
                     send_sem=lent_x_send,
-                    recv_sem=lent_x_recv.at[line],
+                    recv_sem=lent_x_recv.at[line, int(far)],
                     device_id={"tp": tp + 1 - 2 * c},
                     device_id_type=MESH,
                 ).wait_recv()
 
-        lax.fori_loop(0, slots, collect, 0)
-        blocks = [slice(line * CHUNK, (line + 1) * CHUNK) for line in range(2)]
-        for line, rows in enumerate(blocks):
+    def collect_near(part):
+        pl.when(part == 0)(lambda: await_lent(False))
+        for cc in range(2):
+            collect((jnp.where(low_half, 0, 1) + part) * 2 + cc, 0)
+
+    def prepare_lent():
+        await_lent(True)
+        for cc in range(2):
+            collect(far_end * 2 + cc, 0)
+        for line, rows in enumerate(lent_blocks):
             low_rank, inv_rms = normed(lent_l, lent_s, rows)
             weights, total = faded(low_rank, lent_up, lent_bias, jnp.zeros((1, DK), F32))
             lent_fade[rows] = weights
@@ -665,14 +750,20 @@
                 sent_tots[q, line] = total
         for p in range(n_sp):
             give_back(0, p).start()
-        send_reads(LENT_SEQ)
+
+    def work_off():
+        @pl.when(c == sp // 2)
+        def _():
+            for slot in range(relayed, slots - 1):
+                pair_w(slot).wait_recv()
+                pair_w(slot).start()
 
         def multiply(slot, _):
-            @pl.when((c != sp // 2) | (slot >= relayed))
+            @pl.when((c != sp // 2) | (slot == slots - 1))
             def _():
                 pair_w(slot).wait_recv()
 
-            @pl.when((c == sp // 2) & (slot >= relayed))
+            @pl.when((c == sp // 2) & (slot == slots - 1))
             def _():
                 pair_w(slot).start()
 
@@ -681,7 +772,7 @@
             return 0
 
         lax.fori_loop(0, slots, multiply, 0)
-        for line, rows in enumerate(blocks):
+        for line, rows in enumerate(lent_blocks):
             inv_rms = lent_scale[rows, :1]
             keys = (lent_kv[rows, :DK] * inv_rms).astype(BF16).astype(F32)
             weighted = keys * lent_fade[rows]
@@ -689,8 +780,18 @@
             block = jnp.dot(weighted.T.astype(BF16), values, preferred_element_type=F32)
             for p in range(n_sp):
                 lent_terms[p, line] = block[p * share : (p + 1) * share].astype(BF16)
+            lent_state[line] = block
         for p in range(n_sp):
             give_back(1, p).start()
+        ask_copy(c).wait_recv()
+        heard = jnp.zeros((1, DV), F32)
+        for line in range(2):
+            wanted = column(asked[line], 0, DK)
+            heard = heard + jnp.sum(wanted * lent_state[line], axis=0, keepdims=True)
+        for p in range(n_sp):
+            sent_reads[p] = heard
+        for p in range(n_sp):
+            give_back(2, p).start()
 
     def send_hint():
         low_rank, inv_rms = normed(acc_l, acc_s, tail)
@@ -698,16 +799,7 @@
         hint[...] = jnp.concatenate([low_rank, spread], axis=1).T[: hint.shape[0]]
         hint_copy().start()
 
-        def release(i, _):
-            zz = source(i)
-
-            @pl.when((zz >= 0) & (zz < n_z) & held(tail, zz))
-            def _():
-                each_way(tail, zz, lambda copy: copy.start())
-
-            return 0
-
-        lax.fori_loop(1, final_step + 1, release, 0)
+        each_way(tail, far_end, lambda copy: copy.start())
 
     def take_hint():
         hint_copy().wait_recv()
@@ -716,29 +808,13 @@
             [hint[...], jnp.zeros((128 - hint.shape[0], CHUNK), F32)], axis=0
         ).T
         fade_chunk(tail, full[:, :rank], full[:, rank : rank + 1])
-
-        overdue(visit)
-
-    def overdue(act):
-        def one(i, _):
-            zz = source(i)
-
-            @pl.when((zz >= 0) & (zz < n_z))
-            def _():
-                act(i, tail)
-
-            return 0
-
-        lax.fori_loop(2, final_step, one, 0)
+        send_asks()
 
     steps = 2 * n_z - 2
 
     def ready(i, j):
         zz = source(i)
-        inside = (zz >= 0) & (zz < n_z)
-        if lend:
-            inside = inside & jnp.logical_not(at_end & (j == tail) & (i > 1) & (i < final_step))
-        return inside
+        return (zz >= 0) & (zz < n_z)
 
     def settle(i, j):
         final = i == final_step
@@ -746,8 +822,6 @@
 
         @pl.when(ready(i, j))
         def _():
-            if lend:
-                pl.when(at_end & closing)(lambda: overdue(complete))
             complete(i, j)
             if lend:
                 pl.when(at_inner & closing)(send_hint)
@@ -783,6 +857,13 @@
 
                 lax.fori_loop(0, slots, lend_slot, 0)
 
+        if lend:
+            pl.when(at_inner & (i == final_step) & (j == tail))(prepare_lent)
+            part = j - (tail - n_z + 1)
+            pl.when(at_inner & (i == final_step) & (part >= 0) & (j < tail))(
+                lambda: collect_near(part)
+            )
+
         @pl.when(ready(i, j))
         def _():
             visit(i, j)
@@ -802,13 +883,10 @@
         def _():
             work_off()
 
-    rest = [seq for seq in range(seqs) if not (lend and seq == LENT_SEQ)]
-    for seq in rest:
+    for seq in range(seqs):
         send_parts(seq)
-    if lend:
-        pl.when(jnp.logical_not(at_inner))(lambda: send_reads(LENT_SEQ))
-    for seq in rest:
-        sum_terms(seq, False)
+    for seq in range(seqs):
+        sum_terms(seq, lend and seq == LENT_SEQ)
 
     def drained(count, send_sem):
         pltpu.make_async_remote_copy(
@@ -823,12 +901,12 @@
     for plane in range(n_z):
         edge = plane in (0, n_z - 1)
         hops = (0 if plane == 0 else n_z - plane) + (0 if plane == n_z - 1 else plane + 1)
-        hops = hops * chunks
-        pairs = n_z * chunks
+        hops = hops * chunks * CHUNK
+        pairs = n_z * chunks * CHUNK
         if lend and plane in (1, n_z - 2):
-            hops -= n_z - 1
+            hops -= (n_z - 1) * lent_rows
         if lend and edge:
-            pairs -= n_z
+            pairs -= n_z * lent_rows
 
         @pl.when(z == plane)
         def _():
@@ -836,14 +914,26 @@
             drained(pairs, pair_send)
 
     if lend:
-        pl.when(lender)(lambda: w_copy_all(lent_w_send).wait_send())
+
+        @pl.when(lender)
+        def _():
+            w_copy_all(lent_w_send).wait_send()
+            pltpu.make_async_remote_copy(
+                src_ref=asks,
+                dst_ref=asks,
+                send_sem=ask_send,
+                recv_sem=ask_recv,
+                device_id={"tp": inner * 2 + c},
+                device_id_type=MESH,
+            ).wait_send()
 
         @pl.when(at_inner)
         def _():
             pl.when(c == sp // 2)(lambda: w_copy_all(lent_w_pair).wait_send())
-            drained(n_z * (n_sp - 1), lent_x_send)
+            drained(n_z * (n_sp - 1) * lent_rows, lent_x_send)
             given(0).wait_send()
             given(1).wait_send()
+            given(2).wait_send()
             hint_copy().wait_send()
 
     for seq in range(seqs):
@@ -893,29 +983,36 @@
     lent = []
     if lends(n_sp, n_z, heads):
         lent = [
-            pltpu.VMEM((2, n_z, 2, CHUNK, feats), BF16),
+            pltpu.VMEM((2, n_z, 2, CHUNK + EXTRA, feats), BF16),
             pltpu.VMEM((model, DK + DV), BF16),
             pltpu.VMEM((rank, DK), BF16),
             pltpu.VMEM((1, DK), F32),
-            pltpu.VMEM((2 * CHUNK, DK + DV), F32),
-            pltpu.VMEM((2 * CHUNK, rank), F32),
-            pltpu.VMEM((2 * CHUNK, 128), F32),
-            pltpu.VMEM((2 * CHUNK, DK), F32),
-            pltpu.VMEM((2 * CHUNK, DK), F32),
+            pltpu.VMEM((2 * (CHUNK + EXTRA), DK + DV), F32),
+            pltpu.VMEM((2 * (CHUNK + EXTRA), rank), F32),
+            pltpu.VMEM((2 * (CHUNK + EXTRA), 128), F32),
+            pltpu.VMEM((2 * (CHUNK + EXTRA), DK), F32),
+            pltpu.VMEM((2 * (CHUNK + EXTRA), DK), F32),
             pltpu.VMEM((rank + 8, CHUNK), F32),
             pltpu.VMEM((n_sp, 2, share, DV), BF16),
             pltpu.VMEM((n_sp, 2, 1, DK), F32),
             pltpu.VMEM((heads, n_sp, share, DV), BF16),
             pltpu.VMEM((heads, n_sp, 1, DK), F32),
+            pltpu.VMEM((n_sp, 1, DK), F32),
+            pltpu.VMEM((2, 1, DK), F32),
+            pltpu.VMEM((n_sp, 1, DV), F32),
+            pltpu.VMEM((heads, 2, 1, DV), F32),
+            pltpu.VMEM((2, DK, DV), F32),
             dma,
             dma,
             dma,
-            dma((2,)),
+            dma,
+            dma,
+            dma((2, 2)),
             dma,
             dma,
             dma((slots,)),
-            dma((2,)),
-            dma((2,)),
+            dma((3,)),
+            dma((3,)),
         ]
     cache, parts = pl.pallas_call(
         functools.partial(kernel, n_sp, n_z),
@@ -926,7 +1023,7 @@
         in_specs=[hbm] * 8,
         out_specs=(vmem, vmem),
         scratch_shapes=[
-            pltpu.VMEM((chunks * slots, CHUNK, feats), BF16),
+            pltpu.VMEM((chunks * slots * CHUNK, feats), BF16),
             pltpu.VMEM((model, key_cols), BF16),
             pltpu.VMEM((model, value_cols), BF16),
             pltpu.VMEM((rank, model), BF16),

time: 78.5 us -> 74 us (0.943)
  Pallas kernels: 77.7 us -> 73.2 us
    pallas_call x1, Pallas kernels: 76.2 us -> 71.6 us  [per_device(): pl.pallas_call(functools.partial(kernel, n_sp, n_z), out_shape=(jax.Shape...]
where the time goes in v3:
time: 74 us; the launch traced here: 73.8 us
  Pallas kernels  73.2 us (99%)
    pallas_call x1, Pallas kernels, per_device(): pl.pallas_call(functools.partial(kernel, n_sp, n_z), out_shape=(jax.Shape...  71.6 us
    pallas_call x1, Pallas kernels, per_device(): pl.pallas_call(norm_kernel, out_shape=(jax.ShapeDtypeStruct((seqs, heads,...  1.55 us

profile of v3, /device:TPU:0, one launch (start us, length us, event | category | flops | bytes accessed | tf_op | source)
XLA Modules:
  0.0 73.8 jit_solution(7515474889546731179)
XLA Ops:
  0.6 71.6 %shard_map.104 = (bf16[2,2,32,256]{3,2,1,0:T(8,128)(2,1)}, f32[2,4,2,256]{3,2,1,0:T(2,128)}) custom-call(bf16[2,512,512]{2,1,0:T(8,128)(2,1)} %x_ref.1, f32[8,1,512]{2,1,0:T(1,128)} %bitcast.5, bf16[4096,256]{1,0:T(8,128)(2,1)} %wk_hbm.1, bf16[4096,512]{1,0:T(8,128)(2,1)} %wv_hbm.1, bf16[32,4096]{1,0:T(8,128)(2,1)} %bitcast.4, bf16[32,2048]{1,0:T(8,128)(2,1)} %up_hbm.1, ...), custom_call_target="tpu_custom_call" | custom-call | tf_op jit(solution)/shard_map/pallas_call | solution.py:1017
  72.3 1.5 %shard_map.105 = (bf16[2,2,32,256]{3,2,1,0:T(8,128)(2,1)}, bf16[2,512]{1,0:T(2,128)(2,1)}) custom-call(bf16[2,2,32,256]{3,2,1,0:T(8,128)(2,1)} %get-tuple-element.4.cache_in, f32[2,4,2,256]{3,2,1,0:T(2,128)} %get-tuple-element.5.parts_ref, f32[1,256]{1,0:T(1,128)} %bitcast.7), custom_call_target="tpu_custom_call" | custom-call | tf_op jit(solution)/shard_map/pallas_call | solution.py:1072

commit v4 on v3

--- a/solution.py
+++ b/solution.py
@@ -491,15 +491,15 @@
     def fade_chunk(j, low_rank, inv_rms):
         skip = skipped(j) if lend else None
         weights, total = faded(low_rank, up, bias, carry[...], skip)
-        fade[...] = weights
-        scale[...] = jnp.broadcast_to(inv_rms, scale.shape)
+        fade[lax.rem(j, 2)] = weights
+        scale[lax.rem(j, 2)] = jnp.broadcast_to(inv_rms, scale.shape[1:])
         carry[...] = total
 
         @pl.when(lax.rem(j, per_seq) == per_seq - 1)
         def _():
             send_total(j // per_seq)
 
-    def finish_chunk(j):
+    def fade_piece(j):
         seq = j // per_seq
 
         @pl.when(lax.rem(j, per_seq) == 0)
@@ -507,19 +507,26 @@
             carry[...] = jnp.zeros_like(carry)
             state[seq] = jnp.zeros(state.shape[1:], F32)
 
-        last = lax.rem(j, per_seq) == per_seq - 1
+        known = at_end & (j == tail) if lend else j < 0
+
+        @pl.when(used(j) & jnp.logical_not(known))
+        def _():
+            fade_chunk(j, *normed(acc_l, acc_s, j))
+
+        if lend:
+
+            @pl.when(jnp.logical_not(used(j)))
+            def _():
+                send_total(seq)
+
+    def gather_state(j):
+        seq = j // per_seq
 
         @pl.when(used(j))
         def _():
-            known = at_end & (j == tail) if lend else j < 0
-
-            @pl.when(jnp.logical_not(known))
-            def _():
-                fade_chunk(j, *normed(acc_l, acc_s, j))
-
-            inv_rms = scale[:, :1]
+            inv_rms = scale[lax.rem(j, 2)][:, :1]
             keys = (acc_k[j] * inv_rms).astype(BF16).astype(F32)
-            weighted = keys * fade[...]
+            weighted = keys * fade[lax.rem(j, 2)]
             values = (acc_v[j] * inv_rms).astype(BF16)
             for h in range(heads):
                 part = weighted[:, h * DK : (h + 1) * DK].T.astype(BF16)
@@ -528,13 +535,7 @@
                     part, values[:, h * DV : (h + 1) * DV], preferred_element_type=F32
                 )
 
-        if lend:
-
-            @pl.when(jnp.logical_not(used(j)))
-            def _():
-                send_total(seq)
-
-        @pl.when(last)
+        @pl.when(lax.rem(j, per_seq) == per_seq - 1)
         def _():
             send_terms(seq)
 
@@ -816,7 +817,7 @@
         zz = source(i)
         return (zz >= 0) & (zz < n_z)
 
-    def settle(i, j):
+    def settle(i, j, whole=True):
         final = i == final_step
         closing = final & (j == tail)
 
@@ -828,7 +829,9 @@
 
             @pl.when(final)
             def _():
-                finish_chunk(j)
+                fade_piece(j)
+                if whole:
+                    gather_state(j)
 
     def step(t, _):
         i, j = t // chunks, lax.rem(t, chunks)
@@ -838,8 +841,9 @@
 
             @pl.when(early)
             def _():
-                settle(last_i, last_j)
+                settle(last_i, last_j, False)
                 take_hint()
+                gather_state(last_j)
 
             due = (2 * j + 1) // 3
             relaying = at_inner & (c == sp // 2) & (i == final_step) & ((3 * due + 1) // 2 == j)
@@ -1037,8 +1041,8 @@
             pltpu.VMEM((chunks, CHUNK, 128), F32),
             pltpu.VMEM((seqs, key_cols, DV), F32),
             pltpu.VMEM((1, key_cols), F32),
-            pltpu.VMEM((CHUNK, key_cols), F32),
-            pltpu.VMEM((CHUNK, 128), F32),
+            pltpu.VMEM((2, CHUNK, key_cols), F32),
+            pltpu.VMEM((2, CHUNK, 128), F32),
             pltpu.VMEM((seqs, n_sp, 1, key_cols), F32),
             pltpu.VMEM((seqs, n_sp, heads, share, DV), BF16),
             pltpu.VMEM((seqs, n_sp, heads, share, DV), BF16),

time: 74 us -> 74 us (level)
  no operation moved by 1% of the time
where the time goes in v4:
time: 74 us; the launch traced here: 73.8 us
  Pallas kernels  73.2 us (99%)
    pallas_call x1, Pallas kernels, per_device(): pl.pallas_call(functools.partial(kernel, n_sp, n_z), out_shape=(jax.Shape...  71.7 us
    pallas_call x1, Pallas kernels, per_device(): pl.pallas_call(norm_kernel, out_shape=(jax.ShapeDtypeStruct((seqs, heads,...  1.55 us

profile of v4, /device:TPU:0, one launch (start us, length us, event | category | flops | bytes accessed | tf_op | source)
XLA Modules:
  0.0 73.8 jit_solution(16590972183081418305)
XLA Ops:
  0.6 71.7 %shard_map.104 = (bf16[2,2,32,256]{3,2,1,0:T(8,128)(2,1)}, f32[2,4,2,256]{3,2,1,0:T(2,128)}) custom-call(bf16[2,512,512]{2,1,0:T(8,128)(2,1)} %x_ref.1, f32[8,1,512]{2,1,0:T(1,128)} %bitcast.5, bf16[4096,256]{1,0:T(8,128)(2,1)} %wk_hbm.1, bf16[4096,512]{1,0:T(8,128)(2,1)} %wv_hbm.1, bf16[32,4096]{1,0:T(8,128)(2,1)} %bitcast.4, bf16[32,2048]{1,0:T(8,128)(2,1)} %up_hbm.1, ...), custom_call_target="tpu_custom_call" | custom-call | tf_op jit(solution)/shard_map/pallas_call | solution.py:1021
  72.3 1.5 %shard_map.105 = (bf16[2,2,32,256]{3,2,1,0:T(8,128)(2,1)}, bf16[2,512]{1,0:T(2,128)(2,1)}) custom-call(bf16[2,2,32,256]{3,2,1,0:T(8,128)(2,1)} %get-tuple-element.4.cache_in, f32[2,4,2,256]{3,2,1,0:T(2,128)} %get-tuple-element.5.parts_ref, f32[1,256]{1,0:T(1,128)} %bitcast.7), custom_call_target="tpu_custom_call" | custom-call | tf_op jit(solution)/shard_map/pallas_call | solution.py:1076
